TPU v7x, 32 devices: a whole 2x2x4 slice. The times are simulated.
32 devices in a mesh: sp: 8 (over z, x), dp: 4 (over y, core).
Axes of the slice: x: 2, y: 2, z: 4, core: 2. Of those that a mesh axis runs over, the one named last changes fastest.
Arguments:
- residual_in: bfloat16 [4, 1024, 2048], P('dp', 'sp'), may hold values from -6 to 6
- ssm_input: bfloat16 [4, 1024, 2048], P('dp', 'sp'), may hold values from -6 to 6
- state_b: bfloat16 [4, 1024, 2048], P('dp', 'sp'), may hold values from -6 to 6
- state_c: bfloat16 [4, 1024, 2048], P('dp', 'sp'), may hold values from -6 to 6
- step_raw: bfloat16 [4, 1024, 64], P('dp', 'sp'), may hold values from -4 to 3
- gate_input: bfloat16 [4, 1024, 2048], P('dp', 'sp'), may hold values from -6 to 6
- conv_x: float32 [7, 2048], P(None, 'sp'), may hold values from -2 to 2
- conv_b: float32 [7, 2048], P(None, 'sp'), may hold values from -2 to 2
- conv_c: float32 [7, 2048], P(None, 'sp'), may hold values from -2 to 2
- decay_rate: float32 [2, 32], P(None, 'sp'), may hold values from 0 to 1, as said below
- mix_gain: float32 [2048], replicated, may hold values from 0.1 to 1.9
- out_weight: bfloat16 [2048, 2048], P('dp'), may hold values from -0.125 to 0.125
- ffn_gain: float32 [2048], replicated, may hold values from 0.1 to 1.9
- routing: int32 [4, 1024, 4], P('dp', 'sp'), may hold values from 0 to 31, all different within a row; in each aligned block of 128 rows (0 to 127, 128 to 255, ..., all dimensions but the last counted through in order) at most 32 rows name the same one
- route_weight: float32 [4, 1024, 4], P('dp', 'sp'), may hold values from 0.1 to 0.6
- gate_w: bfloat16 [32, 2048, 1024], P(('sp', 'dp')), may hold values from -60 to 60
- up_w: bfloat16 [32, 2048, 1024], P(('sp', 'dp')), may hold values from -60 to 60
- down_w: bfloat16 [32, 1024, 2048], P(('sp', 'dp')), may hold values from -0.1875 to 0.1875
Outputs:
- block_out: bfloat16 [4, 1024, 2048], P('dp', 'sp')
Inputs may be any that keep to these rules, and one draw needn't show every extreme that they name: `routing`: each row names 4 different experts; within the rows of one device no expert is named by more than 32 rows, a bound that some block reaches. `decay_rate`: Positive.
All inputs are finite; a program needn't handle non-finite values.
Results may differ from a plain program's by a relative error of at most 0.0082.
Values may be sent and summed in bfloat16 or wider, within the bound.
A program may use at most 128 MiB of HBM per device.

v0:
```python
import functools

import jax
import jax.numpy as jnp
from jax import lax
from jax.experimental import pallas as pl
from jax.experimental.pallas import tpu as pltpu
from jax.sharding import PartitionSpec as P

HEAD_DIM = 64
STATE = 128
BLOCK = 128
NORM_GROUPS = 4
MESH = pl.DeviceIdType.MESH

highest = lax.Precision.HIGHEST
epsilon = 1e-05
clamp_limit = 7.0
sigmoid_slope = 1.702


def greet(peers):
    barrier = pltpu.get_barrier_semaphore()
    for peer in peers:
        pl.semaphore_signal(barrier, inc=1, device_id=peer, device_id_type=MESH)
    pl.semaphore_wait(barrier, len(peers))


def to_heads_kernel(n, *refs):
    srcs, dsts = refs[:4], refs[4:8]
    bounce, step_bounce, send, recv, local = refs[8:]
    me = lax.axis_index("sp")
    rows = srcs[0].shape[0]
    width = dsts[0].shape[1]
    peers = [lax.rem(me + i, n) for i in range(1, n)]
    greet([{"sp": peer} for peer in peers])
    copies = []
    mine = pl.ds(pl.multiple_of(me * rows, rows), rows)
    for i, peer in enumerate(peers):
        for k in range(4):
            if k < 3:
                part = srcs[k].at[:, pl.ds(pl.multiple_of(peer * width, width), width)]
                there = dsts[k].at[mine, :]
            else:
                part = srcs[k]
                there = dsts[k].at[mine, :]
            copy = pltpu.make_async_remote_copy(
                src_ref=part,
                dst_ref=there,
                send_sem=send.at[i, k],
                recv_sem=recv.at[i, k],
                device_id={"sp": peer},
                device_id_type=MESH,
            )
            copy.start()
            copies.append(copy)
    own = [srcs[k].at[:, pl.ds(pl.multiple_of(me * width, width), width)] for k in range(3)]
    own.append(srcs[3])
    slots = [bounce.at[k] for k in range(3)] + [step_bounce]
    first = [pltpu.make_async_copy(own[k], slots[k], local.at[0, k]) for k in range(4)]
    second = [
        pltpu.make_async_copy(slots[k], dsts[k].at[mine, :], local.at[1, k]) for k in range(4)
    ]
    for k in range(4):
        first[k].start()
    for k in range(4):
        first[k].wait()
        second[k].start()
    for k in range(4):
        second[k].wait()
    for copy in copies:
        copy.wait()


def to_heads(n, arrays, steps):
    rows, full = arrays[0].shape
    width = full // n
    wide = jax.ShapeDtypeStruct((rows * n, width), arrays[0].dtype)
    step_out = jax.ShapeDtypeStruct((rows * n, steps.shape[1]), steps.dtype)
    anywhere = pl.BlockSpec(memory_space=pl.ANY)
    return pl.pallas_call(
        functools.partial(to_heads_kernel, n),
        out_shape=(wide, wide, wide, step_out),
        in_specs=[anywhere] * 4,
        out_specs=(anywhere,) * 4,
        scratch_shapes=[
            pltpu.VMEM((3, rows, width), arrays[0].dtype),
            pltpu.VMEM(steps.shape, steps.dtype),
            pltpu.SemaphoreType.DMA((n - 1, 4)),
            pltpu.SemaphoreType.DMA((n - 1, 4)),
            pltpu.SemaphoreType.DMA((2, 4)),
        ],
        compiler_params=pltpu.CompilerParams(collective_id=1, has_side_effects=True),
        name="to_heads",
    )(*arrays, steps)


def to_tokens_kernel(n, src, dst, bounce, send, recv, local):
    me = lax.axis_index("sp")
    rows = dst.shape[0]
    width = src.shape[1]
    peers = [lax.rem(me + i, n) for i in range(1, n)]
    greet([{"sp": peer} for peer in peers])
    there = dst.at[:, pl.ds(pl.multiple_of(me * width, width), width)]
    copies = []
    for i, peer in enumerate(peers):
        copy = pltpu.make_async_remote_copy(
            src_ref=src.at[pl.ds(pl.multiple_of(peer * rows, rows), rows), :],
            dst_ref=there,
            send_sem=send.at[i],
            recv_sem=recv.at[i],
            device_id={"sp": peer},
            device_id_type=MESH,
        )
        copy.start()
        copies.append(copy)
    first = pltpu.make_async_copy(
        src.at[pl.ds(pl.multiple_of(me * rows, rows), rows), :], bounce, local.at[0]
    )
    first.start()
    first.wait()
    second = pltpu.make_async_copy(bounce, there, local.at[1])
    second.start()
    second.wait()
    for copy in copies:
        copy.wait()


def to_tokens(n, heads):
    length, width = heads.shape
    rows = length // n
    anywhere = pl.BlockSpec(memory_space=pl.ANY)
    return pl.pallas_call(
        functools.partial(to_tokens_kernel, n),
        out_shape=jax.ShapeDtypeStruct((rows, n * width), heads.dtype),
        in_specs=[anywhere],
        out_specs=anywhere,
        scratch_shapes=[
            pltpu.VMEM((rows, width), heads.dtype),
            pltpu.SemaphoreType.DMA((n - 1,)),
            pltpu.SemaphoreType.DMA((n - 1,)),
            pltpu.SemaphoreType.DMA((2,)),
        ],
        compiler_params=pltpu.CompilerParams(collective_id=2, has_side_effects=True),
        name="to_tokens",
    )(heads)


def swap_half_kernel(half, dp_count, src, dst, bounce, send, recv, local):
    n = half * dp_count
    first_sp = lax.axis_index("sp") // half * half
    me = lax.rem(lax.axis_index("sp"), half) * dp_count + lax.axis_index("dp")

    def place(peer):
        return {"sp": first_sp + peer // dp_count, "dp": lax.rem(peer, dp_count)}

    barrier = pltpu.get_barrier_semaphore()

    def call(i, carry):
        peer = lax.rem(me + i, n)
        pl.semaphore_signal(barrier, inc=1, device_id=place(peer), device_id_type=MESH)
        return carry

    lax.fori_loop(1, n, call, 0)
    pl.semaphore_wait(barrier, n - 1)

    def remote(i):
        peer = lax.rem(me + i, n)
        return pltpu.make_async_remote_copy(
            src_ref=src.at[peer],
            dst_ref=dst.at[me],
            send_sem=send.at[i - 1],
            recv_sem=recv.at[i - 1],
            device_id=place(peer),
            device_id_type=MESH,
        )

    def begin(i, carry):
        remote(i).start()
        return carry

    lax.fori_loop(1, n, begin, 0)
    first = pltpu.make_async_copy(src.at[me], bounce, local.at[0])
    first.start()
    first.wait()
    second = pltpu.make_async_copy(bounce, dst.at[me], local.at[1])
    second.start()
    second.wait()

    def finish(i, carry):
        remote(i).wait()
        return carry

    lax.fori_loop(1, n, finish, 0)


def swap_half(half, dp_count, rows, identity):
    n = half * dp_count
    anywhere = pl.BlockSpec(memory_space=pl.ANY)
    return pl.pallas_call(
        functools.partial(swap_half_kernel, half, dp_count),
        out_shape=jax.ShapeDtypeStruct(rows.shape, rows.dtype),
        in_specs=[anywhere],
        out_specs=anywhere,
        scratch_shapes=[
            pltpu.VMEM(rows.shape[1:], rows.dtype),
            pltpu.SemaphoreType.DMA((n - 1,)),
            pltpu.SemaphoreType.DMA((n - 1,)),
            pltpu.SemaphoreType.DMA((2,)),
        ],
        compiler_params=pltpu.CompilerParams(collective_id=identity, has_side_effects=True),
        cost_estimate=pl.CostEstimate(flops=10**11, bytes_accessed=rows.size * 4, transcendentals=0),
        name="swap_half_%d" % identity,
    )(rows)


def mixer_kernel(
    x_ref, b_ref, c_ref, tx_ref, tb_ref, tc_ref, st_ref, stt_ref, rate_ref, ratet_ref,
    o_ref, pad, reads, inside_ref, fade_f, fade_b, sums, carry,
):
    length = x_ref.shape[0]
    lanes = x_ref.shape[1]
    blocks = length // BLOCK
    per_group = st_ref.shape[2] // 2
    taps = tx_ref.shape[0]
    half = taps // 2
    f32, bf16 = jnp.float32, jnp.bfloat16
    for k, ref in enumerate((x_ref, b_ref, c_ref)):
        pad[k, 0:8, :] = jnp.zeros((8, lanes), f32)
        pad[k, length + 8 : length + 16, :] = jnp.zeros((8, lanes), f32)
        pad[k, 8 : length + 8, :] = ref[...].astype(f32)

    def conv(k, taps_ref, base):
        total = None
        for j in range(taps):
            term = pad[k, base + 8 - half + j : base + 8 - half + j + BLOCK, :] * taps_ref[j : j + 1, :]
            total = term if total is None else total + term
        return total * jax.nn.sigmoid(total)

    def softplus(v):
        return jnp.maximum(v, 0.0) + jnp.log(1.0 + jnp.exp(-jnp.abs(v)))

    li = lax.broadcasted_iota(jnp.int32, (BLOCK, BLOCK), 0)
    si = lax.broadcasted_iota(jnp.int32, (BLOCK, BLOCK), 1)
    at_or_after = li >= si
    lower = jnp.where(at_or_after, 1.0, 0.0).astype(f32)
    upper = jnp.where(si >= li, 1.0, 0.0).astype(f32)
    lane_head = lax.broadcasted_iota(jnp.int32, (1, lanes), 1) // HEAD_DIM

    def spread_heads(columns):
        out = columns[0]
        for h in range(1, per_group):
            out = jnp.where(lane_head == h, columns[h], out)
        return jnp.broadcast_to(out, (out.shape[0], lanes))

    for c in range(blocks):
        base = c * BLOCK
        rows = slice(base, base + BLOCK)
        x = conv(0, tx_ref, base)
        write = conv(1, tb_ref, base).astype(bf16)
        read = conv(2, tc_ref, base).astype(bf16)
        reads[rows, :] = read
        dt = softplus(st_ref[0, rows, :])
        dtt = softplus(stt_ref[0, :, rows])
        a = dt * rate_ref[0]
        at = dtt * ratet_ref[0]
        inc = jnp.dot(lower, a, precision=highest, preferred_element_type=f32)
        inct = jnp.dot(at, upper, precision=highest, preferred_element_type=f32)
        exc = inc - a
        exct = inct - at
        tot = inc[BLOCK - 1 : BLOCK, :]
        scores = lax.dot_general(
            read, write, (((1,), (1,)), ((), ())), preferred_element_type=f32
        )
        inside = None
        xb = x.astype(bf16)
        for h in range(per_group):
            f, b = 2 * h, 2 * h + 1
            power = jnp.where(
                at_or_after,
                inct[f : f + 1, :] - inc[:, f : f + 1],
                exc[:, b : b + 1] - exct[b : b + 1, :],
            )
            df, db = dtt[f : f + 1, :], dtt[b : b + 1, :]
            scale = jnp.where(li > si, df, jnp.where(li == si, df + db, db))
            weights = (scores * jnp.exp(power) * scale).astype(bf16)
            xh = jnp.where(lane_head == h, x, 0.0).astype(bf16)
            term = jnp.dot(weights, xh, preferred_element_type=f32)
            inside = term if inside is None else inside + term
        inside_ref[rows, :] = inside
        heads = range(per_group)
        fwd = [inc[:, 2 * h : 2 * h + 1] for h in heads]
        bwd = [exc[:, 2 * h + 1 : 2 * h + 2] for h in heads]
        tot_f = [tot[:, 2 * h : 2 * h + 1] for h in heads]
        tot_b = [tot[:, 2 * h + 1 : 2 * h + 2] for h in heads]
        wf = spread_heads([dt[:, 2 * h : 2 * h + 1] * jnp.exp(fwd[h] - tot_f[h]) for h in heads])
        wb = spread_heads([dt[:, 2 * h + 1 : 2 * h + 2] * jnp.exp(-bwd[h]) for h in heads])
        fade_f[rows, :] = spread_heads([jnp.exp(-fwd[h]) for h in heads])
        fade_b[rows, :] = spread_heads([jnp.exp(bwd[h] - tot_b[h]) for h in heads])
        both = jnp.concatenate([(x * wf).astype(bf16), (x * wb).astype(bf16)], axis=1)
        sums[c] = lax.dot_general(
            write, both, (((0,), (0,)), ((), ())), preferred_element_type=f32
        )
        carry[c : c + 1, :] = jnp.concatenate(
            [
                spread_heads([jnp.exp(-tot_f[h]) for h in heads]),
                spread_heads([jnp.exp(-tot_b[h]) for h in heads]),
            ],
            axis=1,
        )

    state = jnp.zeros((sums.shape[1], lanes), f32)
    for c in range(blocks):
        own = sums[c, :, 0:lanes]
        sums[c, :, 0:lanes] = state
        state = carry[c : c + 1, 0:lanes] * state + own
    state = jnp.zeros((sums.shape[1], lanes), f32)
    for c in reversed(range(blocks)):
        own = sums[c, :, lanes : 2 * lanes]
        sums[c, :, lanes : 2 * lanes] = state
        state = carry[c : c + 1, lanes : 2 * lanes] * state + own
    for c in range(blocks):
        rows = slice(c * BLOCK, (c + 1) * BLOCK)
        moved = jnp.dot(reads[rows, :], sums[c].astype(bf16), preferred_element_type=f32)
        total = (
            inside_ref[rows, :]
            + moved[:, 0:lanes] * fade_f[rows, :]
            + moved[:, lanes : 2 * lanes] * fade_b[rows, :]
        )
        o_ref[rows, :] = total.astype(o_ref.dtype)


def mixer(signal, write, read, conv_x, conv_b, conv_c, steps, rates):
    length, width = signal.shape
    groups = write.shape[1] // STATE
    lanes = width // groups
    columns = steps.shape[1] // groups
    taps = conv_x.shape[0]
    blocks = length // BLOCK
    st = steps.astype(jnp.float32).reshape(length, groups, columns).transpose(1, 0, 2)
    stt = st.transpose(0, 2, 1)
    rate = rates.T.reshape(groups, 1, columns)
    ratet = rates.T.reshape(groups, columns, 1)
    wide = pl.BlockSpec((length, lanes), lambda g: (0, g))
    state = pl.BlockSpec((length, STATE), lambda g: (0, g))
    tap_x = pl.BlockSpec((taps, lanes), lambda g: (0, g))
    tap_s = pl.BlockSpec((taps, STATE), lambda g: (0, g))

    def whole(shape):
        return pl.BlockSpec((1,) + shape, lambda g: (g, 0, 0))

    f32 = jnp.float32
    return pl.pallas_call(
        mixer_kernel,
        grid=(groups,),
        out_shape=jax.ShapeDtypeStruct((length, width), jnp.bfloat16),
        in_specs=[
            wide, state, state, tap_x, tap_s, tap_s,
            whole((length, columns)), whole((columns, length)),
            whole((1, columns)), whole((columns, 1)),
        ],
        out_specs=wide,
        scratch_shapes=[
            pltpu.VMEM((3, length + 16, lanes), f32),
            pltpu.VMEM((length, STATE), jnp.bfloat16),
            pltpu.VMEM((length, lanes), f32),
            pltpu.VMEM((length, lanes), f32),
            pltpu.VMEM((length, lanes), f32),
            pltpu.VMEM((blocks, STATE, 2 * lanes), f32),
            pltpu.VMEM((blocks, 2 * lanes), f32),
        ],
        compiler_params=pltpu.CompilerParams(vmem_limit_bytes=40 * 1024 * 1024),
        cost_estimate=pl.CostEstimate(
            flops=40 * 10**9, bytes_accessed=4 * length * width * 2, transcendentals=0
        ),
        name="mixer",
    )(signal, write, read, conv_x, conv_b, conv_c, st, stt, rate, ratet)


def scale_rows(values, gains):
    return values * lax.rsqrt(jnp.mean(values * values, axis=-1, keepdims=True) + epsilon) * gains


def group_scale(values, gains):
    shaped = values.reshape(values.shape[:-1] + (NORM_GROUPS, values.shape[-1] // NORM_GROUPS))
    shaped = shaped * lax.rsqrt(jnp.mean(shaped * shaped, axis=-1, keepdims=True) + epsilon)
    return shaped.reshape(values.shape) * gains


def expert_apply(rows, gate_mat, up_mat, down_mat):
    gate_value = jnp.minimum(
        jnp.dot(rows, gate_mat, preferred_element_type=jnp.float32), clamp_limit
    )
    up_value = jnp.clip(
        jnp.dot(rows, up_mat, preferred_element_type=jnp.float32), -clamp_limit, clamp_limit
    )
    active = ((up_value + 1.0) * gate_value * jax.nn.sigmoid(sigmoid_slope * gate_value)).astype(
        jnp.bfloat16
    )
    return jnp.dot(active, down_mat, preferred_element_type=jnp.float32).astype(jnp.bfloat16)


def gather_rows(weight, count):
    parts = {0: weight}
    step = count // 2
    while step >= 1:
        pairs = [(d, d ^ step) for d in range(count)]
        for offset, block in list(parts.items()):
            parts[offset ^ step] = lax.ppermute(block, "dp", pairs)
        step //= 2
    return parts


def per_device(
    residual_in, ssm_input, state_b, state_c, step_raw, gate_input, conv_x, conv_b, conv_c,
    decay_rate, mix_gain, out_weight, ffn_gain, routing, route_weight, gate_w, up_w, down_w,
):
    sp_count = lax.axis_size("sp")
    dp_count = lax.axis_size("dp")
    bf16, f32 = jnp.bfloat16, jnp.float32
    half = sp_count // 2
    near = half * dp_count
    mirror = [(i, (i + half) % sp_count) for i in range(sp_count)]
    first_expert = lax.axis_index("sp") // half * near
    far_routing = lax.ppermute(routing[0], "sp", mirror)
    far_weight = lax.ppermute(route_weight[0], "sp", mirror)
    parts = gather_rows(out_weight, dp_count)
    signal, write, read, steps = to_heads(
        sp_count, (ssm_input[0], state_b[0], state_c[0]), step_raw[0]
    )
    columns = steps.shape[1] // sp_count
    steps = lax.dynamic_slice_in_dim(steps, lax.axis_index("sp") * columns, columns, axis=1)
    mixed_heads = mixer(signal, write, read, conv_x, conv_b, conv_c, steps, decay_rate)
    mixed_tokens = to_tokens(sp_count, mixed_heads)

    token_count = residual_in.shape[1]
    model_width = residual_in.shape[2]
    gated = mixed_tokens.astype(f32) * jax.nn.silu(gate_input[0].astype(f32))
    mixed = group_scale(gated, mix_gain).astype(bf16)
    depth = out_weight.shape[0]
    me = lax.axis_index("dp")
    stream = residual_in[0].astype(f32)
    for offset, block in parts.items():
        piece = lax.dynamic_slice_in_dim(mixed, (me ^ offset) * depth, depth, axis=1)
        stream = stream + jnp.dot(piece, block, preferred_element_type=f32)
    ffn_input = scale_rows(stream, ffn_gain).astype(bf16)

    top_count = routing.shape[2]
    capacity = 2 * token_count * top_count // (sp_count * dp_count)
    flat = near * capacity
    earlier = (
        lax.iota(jnp.int32, token_count)[:, None] < lax.iota(jnp.int32, token_count)[None, :]
    ).astype(bf16)

    def tables(names, weights):
        chosen = names.T[:, None, :] == (first_expert + lax.iota(jnp.int32, near))[None, :, None]
        named = jnp.any(chosen, axis=0)
        weight_of = jnp.sum(jnp.where(chosen, weights.T[:, None, :], 0.0), axis=0)
        slot = jnp.dot(named.astype(bf16), earlier, preferred_element_type=f32).astype(jnp.int32)
        slot = jnp.where(named, slot, -1)
        pick = slot[:, None, :] == lax.iota(jnp.int32, capacity)[None, :, None]
        high = weight_of.astype(bf16)
        low = (weight_of - high.astype(f32)).astype(bf16)
        zero = jnp.zeros((), bf16)
        combine = jnp.concatenate(
            [
                jnp.where(pick, high[:, None, :], zero).reshape(flat, token_count),
                jnp.where(pick, low[:, None, :], zero).reshape(flat, token_count),
            ],
            axis=1,
        )
        return pick.astype(bf16).reshape(flat, token_count), combine

    def dispatch(select, tokens, identity):
        outgoing = jnp.dot(select, tokens, preferred_element_type=f32).astype(bf16)
        return swap_half(half, dp_count, outgoing.reshape(near, capacity, model_width), identity)

    def serve(arrived):
        return expert_apply(
            arrived.reshape(flat, model_width), gate_w[0], up_w[0], down_w[0]
        ).reshape(arrived.shape)

    def collect(combine, served, identity):
        returned = swap_half(half, dp_count, served, identity)
        sums = lax.dot_general(
            combine, returned.reshape(flat, model_width), (((0,), (0,)), ((), ())),
            preferred_element_type=f32,
        )
        return sums[:token_count] + sums[token_count:]

    select_own, combine_own = tables(routing[0], route_weight[0])
    select_far, combine_far = tables(far_routing, far_weight)
    far_input = lax.ppermute(ffn_input, "sp", mirror)
    arrived_own = dispatch(select_own, ffn_input, 3)
    arrived_far = dispatch(select_far, far_input, 4)
    part_far = collect(combine_far, serve(arrived_far), 5).astype(bf16)
    part_back = lax.ppermute(part_far, "sp", mirror)
    routed = collect(combine_own, serve(arrived_own), 6)
    return (stream + routed + part_back.astype(f32)).astype(bf16)[None]


def solution(mesh):
    return jax.shard_map(
        per_device,
        mesh=mesh,
        in_specs=(
            P("dp", "sp", None),
            P("dp", "sp", None),
            P("dp", "sp", None),
            P("dp", "sp", None),
            P("dp", "sp", None),
            P("dp", "sp", None),
            P(None, "sp"),
            P(None, "sp"),
            P(None, "sp"),
            P(None, "sp"),
            P(),
            P("dp", None),
            P(),
            P("dp", "sp", None),
            P("dp", "sp", None),
            P(("sp", "dp"), None, None),
            P(("sp", "dp"), None, None),
            P(("sp", "dp"), None, None),
        ),
        out_specs=P("dp", "sp", None),
        check_vma=False,
    )
```

profile of v0, /device:TPU:7, one launch (start us, length us, event | category | flops | bytes accessed | tf_op | source)
XLA Modules:
  0.0 298.7 jit_solution(8774495545729705565)
XLA Ops:
  0.9 2.3 collective-permute-start.3
  4.2 1.4 copy.48
  5.7 36.1 %to_heads.1 = (bf16[1024,256]{1,0:T(8,128)(2,1)}, bf16[1024,256]{1,0:T(8,128)(2,1)}, bf16[1024,256]{1,0:T(8,128)(2,1)}, bf16[1024,64]{1,0:T(8,128)(2,1)}) custom-call(bf16[128,2048]{1,0:T(8,128)(2,1)} %bitcast.112, bf16[128,2048]{1,0:T(8,128)(2,1)} %bitcast.113, bf16[128,2048]{1,0:T(8,128)(2,1)} %bitcast.114, bf16[128,64]{1,0:T(8,128)(2,1)} %bitcast.115), custom_call_target="tpu_custom_call" | custom-call | tf_op jit(solution)/shard_map/to_heads/pallas_call | solution.py:81
  43.7 8.7 %mixer.1.src = bf16[1024,256]{1,0:T(8,128)(2,1)S(1)} custom-call(bf16[1024,256]{1,0:T(8,128)(2,1)S(1)} %copy-done.1, bf16[1024,256]{1,0:T(8,128)(2,1)S(1)} %copy-done.2, bf16[1024,256]{1,0:T(8,128)(2,1)S(1)} %copy-done.3, f32[7,256]{1,0:T(8,128)S(1)} %copy-done.4, f32[7,256]{1,0:T(8,128)S(1)} %copy-done.5, f32[7,256]{1,0:T(8,128)S(1)} %copy-done.6, ...), custom_call_target="tpu_custom_call" | custom-call | flops 40000000000 | bytes 2097152 | tf_op jit(solution)/shard_map/mixer/pallas_call | solution.py:353
  53.2 21.0 %to_tokens.1 = bf16[128,2048]{1,0:T(8,128)(2,1)} custom-call(bf16[1024,256]{1,0:T(8,128)(2,1)} %copy-done), custom_call_target="tpu_custom_call" | custom-call | tf_op jit(solution)/shard_map/to_tokens/pallas_call | solution.py:133
  74.2 1.4 fusion.55
  77.1 2.8 collective-permute-start.2
  80.4 2.0 convolution_add_fusion.2
  84.1 2.0 fusion.51
  86.2 2.0 fusion.18
  88.2 2.1 multiply_reduce_fusion
  92.9 2.0 convolution_convert_fusion.1
  94.9 44.3 %swap_half_3.1 = bf16[16,32,2048]{2,1,0:T(8,128)(2,1)} custom-call(bf16[16,32,2048]{2,1,0:T(8,128)(2,1)} %bitcast.111), custom_call_target="tpu_custom_call" | custom-call | flops 99999997952 | bytes 4194304 | tf_op jit(solution)/shard_map/swap_half_3/pallas_call | solution.py:200
  139.2 6.5 %fusion.10 = f32[512,1024]{1,0:T(8,128)} fusion(bf16[512,2048]{1,0:T(8,128)(2,1)} %bitcast.126, bf16[1,2048,1024]{2,1,0:T(8,128)(2,1)} %param.34), kind=kOutput, calls=%fused_computation.10 | convolution fusion | flops 2147483648 | bytes 8388608 | tf_op jit(solution)/shard_map/dot_general | solution.py:395
  145.8 11.0 %fusion.12 = bf16[512,2048]{1,0:T(8,128)(2,1)} fusion(bf16[1,1024,2048]{2,1,0:T(8,128)(2,1)} %param.35, f32[512,1024]{1,0:T(8,128)} %fusion.10, bf16[512,2048]{1,0:T(8,128)(2,1)} %bitcast.127, bf16[1,2048,1024]{2,1,0:T(8,128)(2,1)} %param.33), kind=kOutput, calls=%fused_computation.12 | convolution fusion | flops 4301258752 | bytes 14680064 | tf_op jit(solution)/shard_map/dot_general | solution.py:400
  156.7 2.0 convolution_convert_fusion
  158.8 34.6 %swap_half_4.1 = bf16[16,32,2048]{2,1,0:T(8,128)(2,1)} custom-call(bf16[16,32,2048]{2,1,0:T(8,128)(2,1)} %bitcast.110), custom_call_target="tpu_custom_call" | custom-call | flops 99999997952 | bytes 4194304 | tf_op jit(solution)/shard_map/swap_half_4/pallas_call | solution.py:200
  193.4 6.6 %fusion.8 = f32[512,1024]{1,0:T(8,128)} fusion(bf16[512,2048]{1,0:T(8,128)(2,1)} %bitcast.128, bf16[1,2048,1024]{2,1,0:T(8,128)(2,1)} %param.34), kind=kOutput, calls=%fused_computation.8 | convolution fusion | flops 2147483648 | bytes 8388608 | tf_op jit(solution)/shard_map/dot_general | solution.py:395
  200.1 10.4 %fusion.15 = bf16[512,2048]{1,0:T(8,128)(2,1)} fusion(bf16[1,1024,2048]{2,1,0:T(8,128)(2,1)} %param.35, f32[512,1024]{1,0:T(8,128)} %fusion.8, bf16[512,2048]{1,0:T(8,128)(2,1)S(1)} %bitcast.129, bf16[1,2048,1024]{2,1,0:T(8,128)(2,1)} %param.33), kind=kOutput, calls=%fused_computation.13 | convolution fusion | flops 4301258752 | bytes 14680064 | tf_op jit(solution)/shard_map/dot_general | solution.py:400
  210.5 34.7 %swap_half_5.1 = bf16[16,32,2048]{2,1,0:T(8,128)(2,1)} custom-call(bf16[16,32,2048]{2,1,0:T(8,128)(2,1)} %bitcast.130), custom_call_target="tpu_custom_call" | custom-call | flops 99999997952 | bytes 4194304 | tf_op jit(solution)/shard_map/swap_half_5/pallas_call | solution.py:200
  245.2 2.3 fusion.42
  247.7 2.3 collective-permute-start.6
  250.0 45.1 %swap_half_6.1 = bf16[16,32,2048]{2,1,0:T(8,128)(2,1)} custom-call(bf16[16,32,2048]{2,1,0:T(8,128)(2,1)} %bitcast.125), custom_call_target="tpu_custom_call" | custom-call | flops 99999997952 | bytes 4194304 | tf_op jit(solution)/shard_map/swap_half_6/pallas_call | solution.py:200
  295.1 2.4 fusion.38
  (80 shorter events, 11.8 us)
Async XLA Ops:
  0.0 84.1 %collective-permute-start.1 = (bf16[512,2048]{1,0:T(8,128)(2,1)}, bf16[512,2048]{1,0:T(8,128)(2,1)}, u32[]{:S(2)}, u32[]{:S(2)}) collective-permute-start(bf16[512,2048]{1,0:T(8,128)(2,1)} %param.29), channel_id=1, source_target_pairs={{0,1},{1,0},{2,3},{3,2},{4,5},{5,4},{6,7},{7,6},{8,9},{9,8},{10,11... | collective-permute-start | bytes 6291464 | tf_op jit(solution)/shard_map/ppermute | solution.py:409
  0.7 76.4 %collective-permute-start = (bf16[512,2048]{1,0:T(8,128)(2,1)}, bf16[512,2048]{1,0:T(8,128)(2,1)}, u32[]{:S(2)}, u32[]{:S(2)}) collective-permute-start(bf16[512,2048]{1,0:T(8,128)(2,1)} %param.29), channel_id=1, source_target_pairs={{0,2},{1,3},{2,0},{3,1},{4,6},{5,7},{6,4},{7,5},{8,10},{9,11},{10,... | collective-permute-start | bytes 6291464 | tf_op jit(solution)/shard_map/ppermute | solution.py:409
  0.9 81.7 %collective-permute-start.3 = (s32[128,4]{0,1:T(4,128)}, s32[128,4]{0,1:T(4,128)S(1)}, u32[]{:S(2)}, u32[]{:S(2)}) collective-permute-start(s32[128,4]{0,1:T(4,128)} %bitcast.116), channel_id=1, source_target_pairs={{0,16},{4,20},{8,24},{12,28},{16,0},{20,4},{24,8},{28,12},{1,17},{... | collective-permute-start | bytes 6152 | tf_op jit(solution)/shard_map/ppermute | solution.py:425
  3.2 79.9 %collective-permute-start.4 = (f32[128,4]{0,1:T(4,128)}, f32[128,4]{0,1:T(4,128)S(1)}, u32[]{:S(2)}, u32[]{:S(2)}) collective-permute-start(f32[128,4]{0,1:T(4,128)} %bitcast.121), channel_id=1, source_target_pairs={{0,16},{4,20},{8,24},{12,28},{16,0},{20,4},{24,8},{28,12},{1,17},{... | collective-permute-start | bytes 6152 | tf_op jit(solution)/shard_map/ppermute | solution.py:426
  3.3 40.3 %copy-start.4 = (f32[7,256]{1,0:T(8,128)S(1)}, f32[7,256]{1,0:T(8,128)}, u32[]{:S(2)}) copy-start(f32[7,256]{1,0:T(8,128)} %tx_ref.1) | copy-start | bytes 21508
  3.3 40.3 %copy-start.5 = (f32[7,256]{1,0:T(8,128)S(1)}, f32[7,256]{1,0:T(8,128)}, u32[]{:S(2)}) copy-start(f32[7,256]{1,0:T(8,128)} %tb_ref.1) | copy-start | bytes 21508
  3.3 40.3 %copy-start.6 = (f32[7,256]{1,0:T(8,128)S(1)}, f32[7,256]{1,0:T(8,128)}, u32[]{:S(2)}) copy-start(f32[7,256]{1,0:T(8,128)} %tc_ref.1) | copy-start | bytes 21508
  41.8 1.8 copy-start.1
  43.6 30.5 %copy-start.10 = (bf16[1,128,2048]{2,1,0:T(8,128)(2,1)S(1)}, bf16[1,128,2048]{2,1,0:T(8,128)(2,1)}, u32[]{:S(2)}) copy-start(bf16[1,128,2048]{2,1,0:T(8,128)(2,1)} %param.23) | copy-start | bytes 1572868
  76.3 3.7 %copy-start.9 = (bf16[128,2048]{1,0:T(8,128)(2,1)S(1)}, bf16[128,2048]{1,0:T(8,128)(2,1)}, u32[]{:S(2)}) copy-start(bf16[128,2048]{1,0:T(8,128)(2,1)} %to_tokens.1) | copy-start | bytes 1572868
  76.3 3.7 %copy-start.16 = (f32[2048]{0:T(1024)S(1)}, f32[2048]{0:T(1024)}, u32[]{:S(2)}) copy-start(f32[2048]{0:T(1024)} %param.28) | copy-start | bytes 24580
  76.7 3.7 %copy-start.15 = (bf16[1,128,2048]{2,1,0:T(8,128)(2,1)S(1)}, bf16[1,128,2048]{2,1,0:T(8,128)(2,1)}, u32[]{:S(2)}) copy-start(bf16[1,128,2048]{2,1,0:T(8,128)(2,1)} %param.18) | copy-start | bytes 1572868
  77.1 11.1 %collective-permute-start.2 = (bf16[512,2048]{1,0:T(8,128)(2,1)}, bf16[512,2048]{1,0:T(8,128)(2,1)}, u32[]{:S(2)}, u32[]{:S(2)}) collective-permute-start(bf16[512,2048]{1,0:T(8,128)(2,1)} %collective-permute-done), channel_id=1, source_target_pairs={{0,1},{1,0},{2,3},{3,2},{4,5},{5,4},{6,7},{7,6},{8,9},{9,8},{10,11... | collective-permute-start | bytes 6291464 | tf_op jit(solution)/shard_map/ppermute | solution.py:409
  80.4 2.2 copy-start.18
  80.4 2.7 copy-start.19
  88.2 3.2 %copy-start.17 = (f32[2048]{0:T(1024)S(1)}, f32[2048]{0:T(1024)}, u32[]{:S(2)}) copy-start(f32[2048]{0:T(1024)} %param.30) | copy-start | bytes 24580
  91.6 65.1 %collective-permute-start.5 = (bf16[128,2048]{1,0:T(8,128)(2,1)S(1)}, bf16[128,2048]{1,0:T(8,128)(2,1)S(1)}, u32[]{:S(2)}, u32[]{:S(2)}) collective-permute-start(bf16[128,2048]{1,0:T(8,128)(2,1)S(1)} %multiply_convert_fusion.2), channel_id=1, source_target_pairs={{0,16},{4,20},{8,24},{12,28},{16,0},{20,4},{24,8},{28,12},{1,17},{... | collective-permute-start | bytes 1572872 | tf_op jit(solution)/shard_map/ppermute | solution.py:493
  193.4 6.7 %copy-start.20 = (bf16[16,32,2048]{2,1,0:T(8,128)(2,1)S(1)}, bf16[16,32,2048]{2,1,0:T(8,128)(2,1)}, u32[]{:S(2)}) copy-start(bf16[16,32,2048]{2,1,0:T(8,128)(2,1)} %swap_half_4.1) | copy-start | bytes 6291460
  210.5 34.8 %copy-start.13 = (bf16[512,128]{1,0:T(8,128)(2,1)S(1)}, bf16[512,128]{1,0:T(8,128)(2,1)}, u32[]{:S(2)}) copy-start(bf16[512,128]{1,0:T(8,128)(2,1)} %get-tuple-element.25) | copy-start | bytes 393220
  210.5 34.8 %copy-start.14 = (bf16[512,128]{1,0:T(8,128)(2,1)S(1)}, bf16[512,128]{1,0:T(8,128)(2,1)}, u32[]{:S(2)}) copy-start(bf16[512,128]{1,0:T(8,128)(2,1)} %get-tuple-element.26) | copy-start | bytes 393220
  247.7 49.9 %collective-permute-start.6 = (bf16[128,2048]{1,0:T(8,128)(2,1)S(1)}, bf16[128,2048]{1,0:T(8,128)(2,1)S(1)}, u32[]{:S(2)}, u32[]{:S(2)}) collective-permute-start(bf16[128,2048]{1,0:T(8,128)(2,1)S(1)} %fusion.29), channel_id=1, source_target_pairs={{0,16},{4,20},{8,24},{12,28},{16,0},{20,4},{24,8},{28,12},{1,17},{... | collective-permute-start | bytes 1572872 | tf_op jit(solution)/shard_map/ppermute | solution.py:497
  250.0 45.2 %copy-start.11 = (bf16[512,128]{1,0:T(8,128)(2,1)S(1)}, bf16[512,128]{1,0:T(8,128)(2,1)}, u32[]{:S(2)}) copy-start(bf16[512,128]{1,0:T(8,128)(2,1)} %get-tuple-element.21) | copy-start | bytes 393220
  250.0 45.2 %copy-start.12 = (bf16[512,128]{1,0:T(8,128)(2,1)S(1)}, bf16[512,128]{1,0:T(8,128)(2,1)}, u32[]{:S(2)}) copy-start(bf16[512,128]{1,0:T(8,128)(2,1)} %get-tuple-element.22) | copy-start | bytes 393220
  295.1 2.4 copy-start.8
  (4 other events, 5.5 us)
where the time goes:
time: 299 us
  Pallas kernels  225 us (75%)
  matrix products  51.8 us (17%)
  starting transfers between devices  9.67 us (3%)
  local copies, waits for them, and re-layouts  6.19 us (2%)
  other arithmetic  5.84 us (2%)
    pallas_call x4, Pallas kernels, swap_half(): pl.pallas_call(functools.partial(swap_half_kernel, half, dp_count), out_s...  159 us
    pallas_call x1, Pallas kernels, to_heads(): pl.pallas_call(functools.partial(to_heads_kernel, n), out_shape=(wide, wi...  36.1 us
    dot_general x2, matrix products, expert_apply(): jnp.dot(active, down_mat, preferred_element_type=jnp.float32)  21.4 us
    pallas_call x1, Pallas kernels, to_tokens(): pl.pallas_call(functools.partial(to_tokens_kernel, n), out_shape=jax.Shap...  21 us
    dot_general x2, matrix products, expert_apply(): jnp.dot(rows, up_mat, preferred_element_type=jnp.float32)  13.2 us
    pallas_call x1, Pallas kernels, mixer(): pl.pallas_call(mixer_kernel, grid=(groups,), out_shape=jax.ShapeDtypeStru...  8.71 us
    dot_general x4, matrix products, per_device(): stream = stream + jnp.dot(piece, block, preferred_element_type=f32)  8.25 us
  transfers between devices with their start and end apart: 7, of which 0 were waited for; matrix products, arithmetic and copies ran while one was open for 12% of the time, Pallas kernels for 52%

commit v1 on v0

--- a/solution.py
+++ b/solution.py
@@ -146,72 +146,322 @@
     )(heads)
 
 
-def swap_half_kernel(half, dp_count, src, dst, bounce, send, recv, local):
-    n = half * dp_count
-    first_sp = lax.axis_index("sp") // half * half
-    me = lax.rem(lax.axis_index("sp"), half) * dp_count + lax.axis_index("dp")
-
-    def place(peer):
-        return {"sp": first_sp + peer // dp_count, "dp": lax.rem(peer, dp_count)}
+def plane_order(z, planes, s):
+    below, above = z, planes - 1 - z
+    both = jnp.minimum(below, above)
+    near = (s + 1) // 2
+    from_below = jnp.where(s <= 2 * both, s % 2, jnp.where(below > above, 1, 0))
+    hops = jnp.where(s <= 2 * both, near, s - both)
+    return hops, from_below, z + hops * (1 - 2 * from_below)
+
+
+def experts_kernel(
+    planes, inner, dp_count, top, x_ref, info_ref, gate_hbm, up_hbm, down_hbm, out_ref,
+    gate, up, down, tok, infos, rows_out, rows_in, made, back, high, low, active, part, part_in,
+    wsem, isend, irecv, zsend, zrecv, dsend, drecv, rsend, rrecv, psend, precv, local,
+):
+    f32, bf16 = jnp.float32, jnp.bfloat16
+    near = inner * dp_count
+    tokens, width = x_ref.shape
+    cap = rows_out.shape[2]
+    sp, dp = lax.axis_index("sp"), lax.axis_index("dp")
+    z, x = sp // inner, lax.rem(sp, inner)
+    me = x * dp_count + dp
+
+    def place(p):
+        return {"sp": z * inner + p // dp_count, "dp": lax.rem(p, dp_count)}
+
+    def plane(other):
+        return {"sp": other * inner + x, "dp": dp}
 
     barrier = pltpu.get_barrier_semaphore()
 
     def call(i, carry):
-        peer = lax.rem(me + i, n)
+        peer = lax.rem(me + i, near)
         pl.semaphore_signal(barrier, inc=1, device_id=place(peer), device_id_type=MESH)
         return carry
 
-    lax.fori_loop(1, n, call, 0)
-    pl.semaphore_wait(barrier, n - 1)
-
-    def remote(i):
-        peer = lax.rem(me + i, n)
+    lax.fori_loop(1, near, call, 0)
+    for i in range(1, planes):
+        pl.semaphore_signal(
+            barrier, inc=1, device_id=plane(lax.rem(z + i, planes)), device_id_type=MESH
+        )
+    loads = [
+        pltpu.make_async_copy(gate_hbm.at[0], gate, wsem.at[0]),
+        pltpu.make_async_copy(up_hbm.at[0], up, wsem.at[1]),
+        pltpu.make_async_copy(down_hbm.at[0], down, wsem.at[2]),
+    ]
+    for load in loads:
+        load.start()
+    pl.semaphore_wait(barrier, near - 1 + planes - 1)
+
+    def tell(i):
         return pltpu.make_async_remote_copy(
-            src_ref=src.at[peer],
-            dst_ref=dst.at[me],
-            send_sem=send.at[i - 1],
-            recv_sem=recv.at[i - 1],
+            src_ref=info_ref,
+            dst_ref=infos.at[z],
+            send_sem=isend.at[i],
+            recv_sem=irecv.at[i],
+            device_id=plane(lax.rem(z + i, planes)),
+            device_id_type=MESH,
+        )
+
+    for i in range(1, planes):
+        tell(i).start()
+
+    def along(src, block, step, way):
+        return pltpu.make_async_remote_copy(
+            src_ref=src,
+            dst_ref=tok.at[block],
+            send_sem=zsend.at[way, step],
+            recv_sem=zrecv.at[way, step],
+            device_id=plane(z + 1 - 2 * way),
+            device_id_type=MESH,
+        )
+
+    up_open, down_open = z < planes - 1, z > 0
+
+    @pl.when(up_open)
+    def _():
+        along(x_ref, z, 0, 0).start()
+
+    @pl.when(down_open)
+    def _():
+        along(x_ref, z, 0, 1).start()
+
+    ti = lax.broadcasted_iota(jnp.int32, (tokens, tokens), 0)
+    tj = lax.broadcasted_iota(jnp.int32, (tokens, tokens), 1)
+    earlier = jnp.where(ti < tj, 1.0, 0.0).astype(bf16)
+    expert = (z * near + lax.broadcasted_iota(jnp.int32, (near, tokens), 0)).astype(f32)
+    place_in = lax.broadcasted_iota(jnp.int32, (near, cap, tokens), 1).astype(f32)
+
+    def send_rows(block, i):
+        peer = lax.rem(me + i, near)
+        return pltpu.make_async_remote_copy(
+            src_ref=rows_out.at[block, peer],
+            dst_ref=rows_in.at[block, me],
+            send_sem=dsend.at[block, i],
+            recv_sem=drecv.at[block, i],
             device_id=place(peer),
             device_id_type=MESH,
         )
 
-    def begin(i, carry):
-        remote(i).start()
-        return carry
-
-    lax.fori_loop(1, n, begin, 0)
-    first = pltpu.make_async_copy(src.at[me], bounce, local.at[0])
-    first.start()
-    first.wait()
-    second = pltpu.make_async_copy(bounce, dst.at[me], local.at[1])
-    second.start()
-    second.wait()
-
-    def finish(i, carry):
-        remote(i).wait()
-        return carry
-
-    lax.fori_loop(1, n, finish, 0)
-
-
-def swap_half(half, dp_count, rows, identity):
-    n = half * dp_count
+    def keep_rows(block):
+        return pltpu.make_async_copy(
+            rows_out.at[block, me], rows_in.at[block, me], local.at[0, block]
+        )
+
+    def send_back(block, i):
+        peer = lax.rem(me + i, near)
+        return pltpu.make_async_remote_copy(
+            src_ref=made.at[block, peer],
+            dst_ref=back.at[block, me],
+            send_sem=rsend.at[block, i],
+            recv_sem=rrecv.at[block, i],
+            device_id=place(peer),
+            device_id_type=MESH,
+        )
+
+    def keep_back(block):
+        return pltpu.make_async_copy(made.at[block, me], back.at[block, me], local.at[1, block])
+
+    def each(what):
+        def one(i, carry):
+            what(i)
+            return carry
+
+        lax.fori_loop(1, near, one, 0)
+
+    def dispatch(block, values, info):
+        names, weights = info[0:top, :], info[top : 2 * top, :]
+        named, weight = None, None
+        for k in range(top):
+            hit = names[k : k + 1, :] == expert
+            one = jnp.where(hit, 1.0, 0.0)
+            share = jnp.where(hit, weights[k : k + 1, :], 0.0)
+            named = one if named is None else named + one
+            weight = share if weight is None else weight + share
+        slot = jnp.dot(named.astype(bf16), earlier, preferred_element_type=f32)
+        slot = jnp.where(named > 0.5, slot, -1.0)
+        pick = slot[:, None, :] == place_in
+        rough = weight.astype(bf16).astype(f32)
+        rest = weight - rough
+
+        def table(v):
+            return jnp.where(pick, v, 0.0).reshape(near * cap, tokens).astype(bf16)
+
+        high[block] = table(rough[:, None, :])
+        low[block] = table(rest[:, None, :])
+        select = table(jnp.ones((near, 1, tokens), f32))
+        chunk = 512
+        for at in range(0, width, chunk):
+            rows = jnp.dot(select, values[:, at : at + chunk], preferred_element_type=f32)
+            rows_out[block, :, :, at : at + chunk] = rows.astype(bf16).reshape(near, cap, chunk)
+        each(lambda i: send_rows(block, i).start())
+        keep_rows(block).start()
+
+    def arrive(s):
+        hops, from_below, block = plane_order(z, planes, s)
+        way = 1 - from_below
+        along(tok.at[block], block, hops - 1, way).wait_recv()
+        onward = jnp.where(from_below == 1, z + 1, z - 1)
+
+        @pl.when((onward >= 0) & (onward < planes))
+        def _():
+            along(tok.at[block], block, hops, way).start()
+
+        source = lax.rem(z - block + planes, planes)
+        tell(source).wait_recv()
+        dispatch(block, tok[block], infos[block])
+        return block
+
+    hidden = gate.shape[1]
+    flat = near * cap
+
+    def serve(block):
+        keep_rows(block).wait()
+        each(lambda i: send_rows(block, i).wait_recv())
+        tile = 256
+
+        def lift(n, carry):
+            cols = pl.ds(pl.multiple_of(n * tile, tile), tile)
+            rows = rows_in[block].reshape(flat, width)
+            g = jnp.minimum(jnp.dot(rows, gate[:, cols], preferred_element_type=f32), clamp_limit)
+            u = jnp.dot(rows, up[:, cols], preferred_element_type=f32)
+            u = jnp.clip(u, -clamp_limit, clamp_limit)
+            active[:, cols] = ((u + 1.0) * g * jax.nn.sigmoid(sigmoid_slope * g)).astype(bf16)
+            return carry
+
+        lax.fori_loop(0, hidden // tile, lift, 0)
+
+        def lower(n, carry):
+            cols = pl.ds(pl.multiple_of(n * tile, tile), tile)
+            y = jnp.dot(active[...], down[:, cols], preferred_element_type=f32)
+            made[block, :, :, cols] = y.astype(bf16).reshape(near, cap, tile)
+            return carry
+
+        lax.fori_loop(0, width // tile, lower, 0)
+
+    def give(block):
+        each(lambda i: send_back(block, i).start())
+        keep_back(block).start()
+
+    def gathered(block, at, chunk):
+        rows = back[block, :, :, at : at + chunk].reshape(flat, chunk)
+        dims = (((0,), (0,)), ((), ()))
+        return lax.dot_general(
+            high[block], rows, dims, preferred_element_type=f32
+        ) + lax.dot_general(low[block], rows, dims, preferred_element_type=f32)
+
+    def send_part(block, i):
+        return pltpu.make_async_remote_copy(
+            src_ref=part.at[block],
+            dst_ref=part_in.at[z],
+            send_sem=psend.at[i],
+            recv_sem=precv.at[i],
+            device_id=plane(block),
+            device_id_type=MESH,
+        )
+
+    def landed(block):
+        keep_back(block).wait()
+        each(lambda i: send_back(block, i).wait_recv())
+
+    def collect(block):
+        landed(block)
+        chunk = 512
+        for at in range(0, width, chunk):
+            part[block, :, at : at + chunk] = gathered(block, at, chunk).astype(bf16)
+        send_part(block, lax.rem(block - z + planes, planes)).start()
+
+    blocks = [z]
+    dispatch(z, x_ref[...], info_ref[...])
+    served = 0
+    for s in range(1, planes):
+        blocks.append(arrive(s))
+        if s == planes - 2:
+            for load in loads:
+                load.wait()
+            serve(blocks[0])
+            served = 1
+    if not served:
+        for load in loads:
+            load.wait()
+        serve(blocks[0])
+    for s in range(1, planes):
+        serve(blocks[s])
+        give(blocks[s])
+    give(blocks[0])
+    for s in range(1, planes):
+        collect(blocks[s])
+    landed(z)
+    chunk = 512
+    for at in range(0, width, chunk):
+        out_ref[:, at : at + chunk] = gathered(z, at, chunk)
+    for i in range(1, planes):
+        send_part(lax.rem(z + i, planes), i).wait_recv()
+        out_ref[...] += part_in[lax.rem(z - i + planes, planes)].astype(f32)
+
+    for i in range(1, planes):
+        tell(i).wait_send()
+        send_part(lax.rem(z + i, planes), i).wait_send()
+    for block in range(planes):
+        each(lambda i: send_rows(block, i).wait_send())
+        each(lambda i: send_back(block, i).wait_send())
+
+    @pl.when(up_open)
+    def _():
+        along(x_ref, z, 0, 0).wait_send()
+
+    @pl.when(down_open)
+    def _():
+        along(x_ref, z, 0, 1).wait_send()
+
+    for step in range(1, planes):
+
+        @pl.when(up_open & (z - step >= 0))
+        def _():
+            along(tok.at[z], z, step, 0).wait_send()
+
+        @pl.when(down_open & (z + step < planes))
+        def _():
+            along(tok.at[z], z, step, 1).wait_send()
+
+
+def experts(planes, inner, dp_count, cap, top, tokens_in, info, gate_w, up_w, down_w):
+    near = inner * dp_count
+    tokens, width = tokens_in.shape
+    hidden = gate_w.shape[2]
+    bf16, f32 = jnp.bfloat16, jnp.float32
     anywhere = pl.BlockSpec(memory_space=pl.ANY)
+    inside = pl.BlockSpec(memory_space=pltpu.VMEM)
+    dma = pltpu.SemaphoreType.DMA
+    rows = pltpu.VMEM((planes, near, cap, width), bf16)
+    table = pltpu.VMEM((planes, near * cap, tokens), bf16)
+    blocks = pltpu.VMEM((planes, tokens, width), bf16)
     return pl.pallas_call(
-        functools.partial(swap_half_kernel, half, dp_count),
-        out_shape=jax.ShapeDtypeStruct(rows.shape, rows.dtype),
-        in_specs=[anywhere],
-        out_specs=anywhere,
+        functools.partial(experts_kernel, planes, inner, dp_count, top),
+        out_shape=jax.ShapeDtypeStruct((tokens, width), f32),
+        in_specs=[inside, inside, anywhere, anywhere, anywhere],
+        out_specs=inside,
         scratch_shapes=[
-            pltpu.VMEM(rows.shape[1:], rows.dtype),
-            pltpu.SemaphoreType.DMA((n - 1,)),
-            pltpu.SemaphoreType.DMA((n - 1,)),
-            pltpu.SemaphoreType.DMA((2,)),
+            pltpu.VMEM((width, hidden), bf16),
+            pltpu.VMEM((width, hidden), bf16),
+            pltpu.VMEM((hidden, width), bf16),
+            blocks,
+            pltpu.VMEM((planes,) + info.shape, f32),
+            rows, rows, rows, rows, table, table,
+            pltpu.VMEM((near * cap, hidden), bf16),
+            blocks, blocks,
+            dma((3,)), dma((planes,)), dma((planes,)), dma((2, planes)), dma((2, planes)),
+            dma((planes, near)), dma((planes, near)), dma((planes, near)), dma((planes, near)),
+            dma((planes,)), dma((planes,)), dma((2, planes)),
         ],
-        compiler_params=pltpu.CompilerParams(collective_id=identity, has_side_effects=True),
-        cost_estimate=pl.CostEstimate(flops=10**11, bytes_accessed=rows.size * 4, transcendentals=0),
-        name="swap_half_%d" % identity,
-    )(rows)
+        compiler_params=pltpu.CompilerParams(
+            collective_id=3, has_side_effects=True, vmem_limit_bytes=60 * 1024 * 1024
+        ),
+        cost_estimate=pl.CostEstimate(flops=10**11, bytes_accessed=10**8, transcendentals=0),
+        name="experts",
+    )(tokens_in, info, gate_w, up_w, down_w)
 
 
 def mixer_kernel(
@@ -387,19 +637,6 @@
     return shaped.reshape(values.shape) * gains
 
 
-def expert_apply(rows, gate_mat, up_mat, down_mat):
-    gate_value = jnp.minimum(
-        jnp.dot(rows, gate_mat, preferred_element_type=jnp.float32), clamp_limit
-    )
-    up_value = jnp.clip(
-        jnp.dot(rows, up_mat, preferred_element_type=jnp.float32), -clamp_limit, clamp_limit
-    )
-    active = ((up_value + 1.0) * gate_value * jax.nn.sigmoid(sigmoid_slope * gate_value)).astype(
-        jnp.bfloat16
-    )
-    return jnp.dot(active, down_mat, preferred_element_type=jnp.float32).astype(jnp.bfloat16)
-
-
 def gather_rows(weight, count):
     parts = {0: weight}
     step = count // 2
@@ -418,12 +655,6 @@
     sp_count = lax.axis_size("sp")
     dp_count = lax.axis_size("dp")
     bf16, f32 = jnp.bfloat16, jnp.float32
-    half = sp_count // 2
-    near = half * dp_count
-    mirror = [(i, (i + half) % sp_count) for i in range(sp_count)]
-    first_expert = lax.axis_index("sp") // half * near
-    far_routing = lax.ppermute(routing[0], "sp", mirror)
-    far_weight = lax.ppermute(route_weight[0], "sp", mirror)
     parts = gather_rows(out_weight, dp_count)
     signal, write, read, steps = to_heads(
         sp_count, (ssm_input[0], state_b[0], state_c[0]), step_raw[0]
@@ -446,57 +677,14 @@
     ffn_input = scale_rows(stream, ffn_gain).astype(bf16)
 
     top_count = routing.shape[2]
-    capacity = 2 * token_count * top_count // (sp_count * dp_count)
-    flat = near * capacity
-    earlier = (
-        lax.iota(jnp.int32, token_count)[:, None] < lax.iota(jnp.int32, token_count)[None, :]
-    ).astype(bf16)
-
-    def tables(names, weights):
-        chosen = names.T[:, None, :] == (first_expert + lax.iota(jnp.int32, near))[None, :, None]
-        named = jnp.any(chosen, axis=0)
-        weight_of = jnp.sum(jnp.where(chosen, weights.T[:, None, :], 0.0), axis=0)
-        slot = jnp.dot(named.astype(bf16), earlier, preferred_element_type=f32).astype(jnp.int32)
-        slot = jnp.where(named, slot, -1)
-        pick = slot[:, None, :] == lax.iota(jnp.int32, capacity)[None, :, None]
-        high = weight_of.astype(bf16)
-        low = (weight_of - high.astype(f32)).astype(bf16)
-        zero = jnp.zeros((), bf16)
-        combine = jnp.concatenate(
-            [
-                jnp.where(pick, high[:, None, :], zero).reshape(flat, token_count),
-                jnp.where(pick, low[:, None, :], zero).reshape(flat, token_count),
-            ],
-            axis=1,
-        )
-        return pick.astype(bf16).reshape(flat, token_count), combine
-
-    def dispatch(select, tokens, identity):
-        outgoing = jnp.dot(select, tokens, preferred_element_type=f32).astype(bf16)
-        return swap_half(half, dp_count, outgoing.reshape(near, capacity, model_width), identity)
-
-    def serve(arrived):
-        return expert_apply(
-            arrived.reshape(flat, model_width), gate_w[0], up_w[0], down_w[0]
-        ).reshape(arrived.shape)
-
-    def collect(combine, served, identity):
-        returned = swap_half(half, dp_count, served, identity)
-        sums = lax.dot_general(
-            combine, returned.reshape(flat, model_width), (((0,), (0,)), ((), ())),
-            preferred_element_type=f32,
-        )
-        return sums[:token_count] + sums[token_count:]
-
-    select_own, combine_own = tables(routing[0], route_weight[0])
-    select_far, combine_far = tables(far_routing, far_weight)
-    far_input = lax.ppermute(ffn_input, "sp", mirror)
-    arrived_own = dispatch(select_own, ffn_input, 3)
-    arrived_far = dispatch(select_far, far_input, 4)
-    part_far = collect(combine_far, serve(arrived_far), 5).astype(bf16)
-    part_back = lax.ppermute(part_far, "sp", mirror)
-    routed = collect(combine_own, serve(arrived_own), 6)
-    return (stream + routed + part_back.astype(f32)).astype(bf16)[None]
+    inner = dp_count // 2
+    planes = sp_count // inner
+    capacity = 4 * token_count * top_count // (2 * sp_count * dp_count)
+    info = jnp.concatenate([routing[0].T.astype(f32), route_weight[0].T], axis=0)
+    routed = experts(
+        planes, inner, dp_count, capacity, top_count, ffn_input, info, gate_w, up_w, down_w
+    )
+    return (stream + routed).astype(bf16)[None]
 
 
 def solution(mesh):

time: 299 us -> 216 us (0.72)
  the two profiles are of different devices: /device:TPU:7 before, /device:TPU:29 now
where the time goes in v1:
time: 216 us
  Pallas kernels  190 us (88%)
  other arithmetic  6.9 us (3%)
  matrix products  6.72 us (3%)
  starting transfers between devices  5.88 us (3%)
  local copies, waits for them, and re-layouts  5.67 us (3%)
    pallas_call x1, Pallas kernels, experts(): pl.pallas_call(functools.partial(experts_kernel, planes, inner, dp_count,...  126 us
    pallas_call x1, Pallas kernels, to_heads(): pl.pallas_call(functools.partial(to_heads_kernel, n), out_shape=(wide, wi...  39.2 us
    pallas_call x1, Pallas kernels, to_tokens(): pl.pallas_call(functools.partial(to_tokens_kernel, n), out_shape=jax.Shap...  15.8 us
    pallas_call x1, Pallas kernels, mixer(): pl.pallas_call(mixer_kernel, grid=(groups,), out_shape=jax.ShapeDtypeStru...  8.71 us
    dot_general x4, matrix products, per_device(): stream = stream + jnp.dot(piece, block, preferred_element_type=f32)  6.72 us
    ppermute x3, starting transfers between devices, gather_rows(): parts[offset ^ step] = lax.ppermute(block, 'dp', pairs)  5.88 us
  transfers between devices with their start and end apart: 3, of which 0 were waited for; matrix products, arithmetic and copies ran while one was open for 6% of the time, Pallas kernels for 30%

profile of v1, /device:TPU:29, one launch (start us, length us, event | category | flops | bytes accessed | tf_op | source)
XLA Modules:
  0.0 215.6 jit_solution(8082571651133100128)
XLA Ops:
  0.0 0.7 collective-permute-start.1
  0.7 0.2 collective-permute-start
  0.9 0.8 copy.43
  1.9 1.4 copy.41
  3.3 39.2 %to_heads.1 = (bf16[1024,256]{1,0:T(8,128)(2,1)}, bf16[1024,256]{1,0:T(8,128)(2,1)}, bf16[1024,256]{1,0:T(8,128)(2,1)}, bf16[1024,64]{1,0:T(8,128)(2,1)}) custom-call(bf16[128,2048]{1,0:T(8,128)(2,1)} %bitcast.40, bf16[128,2048]{1,0:T(8,128)(2,1)} %bitcast.41, bf16[128,2048]{1,0:T(8,128)(2,1)} %bitcast.42, bf16[128,64]{1,0:T(8,128)(2,1)} %bitcast.43), custom_call_target="tpu_custom_call" | custom-call | tf_op jit(solution)/shard_map/to_heads/pallas_call | solution.py:81
  42.5 1.2 dynamic-slice_convert_fusion
  43.9 0.4 copy.45.st_ref
  44.4 8.7 %mixer.1.src = bf16[1024,256]{1,0:T(8,128)(2,1)S(1)} custom-call(bf16[1024,256]{1,0:T(8,128)(2,1)S(1)} %copy-done.1, bf16[1024,256]{1,0:T(8,128)(2,1)S(1)} %copy-done.2, bf16[1024,256]{1,0:T(8,128)(2,1)S(1)} %copy-done.3, f32[7,256]{1,0:T(8,128)S(1)} %copy-done.4, f32[7,256]{1,0:T(8,128)S(1)} %copy-done.5, f32[7,256]{1,0:T(8,128)S(1)} %copy-done.6, ...), custom_call_target="tpu_custom_call" | custom-call | flops 40000000000 | bytes 2097152 | tf_op jit(solution)/shard_map/mixer/pallas_call | solution.py:603
  53.1 0.8 copy-done
  53.9 15.8 %to_tokens.1 = bf16[128,2048]{1,0:T(8,128)(2,1)} custom-call(bf16[1024,256]{1,0:T(8,128)(2,1)} %copy-done), custom_call_target="tpu_custom_call" | custom-call | tf_op jit(solution)/shard_map/to_tokens/pallas_call | solution.py:133
  69.7 5.0 %collective-permute-start.2 = (bf16[512,2048]{1,0:T(8,128)(2,1)}, bf16[512,2048]{1,0:T(8,128)(2,1)}, u32[]{:S(2)}, u32[]{:S(2)}) collective-permute-start(bf16[512,2048]{1,0:T(8,128)(2,1)} %collective-permute-done), channel_id=1, source_target_pairs={{0,1},{1,0},{2,3},{3,2},{4,5},{5,4},{6,7},{7,6},{8,9},{9,8},{10,11... | collective-permute-start | bytes 6291464 | tf_op jit(solution)/shard_map/ppermute | solution.py:646
  74.7 1.4 fusion.11
  76.1 0.7 mul.70
  77.3 0.3 copy.50
  77.8 0.6 pad_maximum_fusion.info_ref
  78.4 0.4 multiply_convert_fusion.1
  78.8 0.6 copy-done.8
  79.4 0.5 convolution_add_fusion.2
  79.9 2.0 fusion.7
  81.9 2.1 fusion
  84.0 2.2 multiply_reduce_fusion
  86.2 1.0 multiply_convert_fusion.x_ref
  87.2 126.3 %experts.1 = f32[128,2048]{1,0:T(8,128)} custom-call(bf16[128,2048]{1,0:T(8,128)(2,1)} %multiply_convert_fusion.x_ref, f32[8,128]{1,0:T(8,128)} %pad_maximum_fusion.info_ref, bf16[1,2048,1024]{2,1,0:T(8,128)(2,1)} %gate_hbm.1, bf16[1,2048,1024]{2,1,0:T(8,128)(2,1)} %up_hbm.1, bf16[1,1024,2048]{2,1,0:T(8,128)(2,1)} %down_hbm.1), custom_call_target="tpu_custom_call" | custom-call | flops 99999997952 | bytes 100000000 | tf_op jit(solution)/shard_map/experts/pallas_call | solution.py:441
  213.5 2.1 fusion.5
  (40 shorter events, 0.9 us)
Async XLA Ops:
  0.0 79.9 %collective-permute-start.1 = (bf16[512,2048]{1,0:T(8,128)(2,1)}, bf16[512,2048]{1,0:T(8,128)(2,1)}, u32[]{:S(2)}, u32[]{:S(2)}) collective-permute-start(bf16[512,2048]{1,0:T(8,128)(2,1)} %param.29), channel_id=1, source_target_pairs={{0,1},{1,0},{2,3},{3,2},{4,5},{5,4},{6,7},{7,6},{8,9},{9,8},{10,11... | collective-permute-start | bytes 6291464 | tf_op jit(solution)/shard_map/ppermute | solution.py:646
  0.7 69.1 %collective-permute-start = (bf16[512,2048]{1,0:T(8,128)(2,1)}, bf16[512,2048]{1,0:T(8,128)(2,1)}, u32[]{:S(2)}, u32[]{:S(2)}) collective-permute-start(bf16[512,2048]{1,0:T(8,128)(2,1)} %param.29), channel_id=1, source_target_pairs={{0,2},{1,3},{2,0},{3,1},{4,6},{5,7},{6,4},{7,5},{8,10},{9,11},{10,... | collective-permute-start | bytes 6291464 | tf_op jit(solution)/shard_map/ppermute | solution.py:646
  0.9 43.4 %copy-start.4 = (f32[7,256]{1,0:T(8,128)S(1)}, f32[7,256]{1,0:T(8,128)}, u32[]{:S(2)}) copy-start(f32[7,256]{1,0:T(8,128)} %tx_ref.1) | copy-start | bytes 21508
  0.9 43.4 %copy-start.5 = (f32[7,256]{1,0:T(8,128)S(1)}, f32[7,256]{1,0:T(8,128)}, u32[]{:S(2)}) copy-start(f32[7,256]{1,0:T(8,128)} %tb_ref.1) | copy-start | bytes 21508
  0.9 43.4 %copy-start.6 = (f32[7,256]{1,0:T(8,128)S(1)}, f32[7,256]{1,0:T(8,128)}, u32[]{:S(2)}) copy-start(f32[7,256]{1,0:T(8,128)} %tc_ref.1) | copy-start | bytes 21508
  42.5 1.8 copy-start.1
  42.5 1.8 copy-start.2
  42.5 1.8 copy-start.3
  44.4 30.4 %copy-start.9 = (bf16[1,128,2048]{2,1,0:T(8,128)(2,1)S(1)}, bf16[1,128,2048]{2,1,0:T(8,128)(2,1)}, u32[]{:S(2)}) copy-start(bf16[1,128,2048]{2,1,0:T(8,128)(2,1)} %param.23) | copy-start | bytes 1572868
  53.1 0.8 copy-start
  69.7 14.3 %collective-permute-start.2 = (bf16[512,2048]{1,0:T(8,128)(2,1)}, bf16[512,2048]{1,0:T(8,128)(2,1)}, u32[]{:S(2)}, u32[]{:S(2)}) collective-permute-start(bf16[512,2048]{1,0:T(8,128)(2,1)} %collective-permute-done), channel_id=1, source_target_pairs={{0,1},{1,0},{2,3},{3,2},{4,5},{5,4},{6,7},{7,6},{8,9},{9,8},{10,11... | collective-permute-start | bytes 6291464 | tf_op jit(solution)/shard_map/ppermute | solution.py:646
  76.8 0.9 copy-start.13
  76.8 0.9 copy-start.14
  76.9 1.5 copy-start.7
  76.9 1.5 copy-start.11
  77.3 1.4 copy-start.10
  77.7 1.7 copy-start.8
  84.0 2.2 %copy-start.12 = (f32[2048]{0:T(1024)S(1)}, f32[2048]{0:T(1024)}, u32[]{:S(2)}) copy-start(f32[2048]{0:T(1024)} %param.30) | copy-start | bytes 24580

commit v2 on v1

--- a/solution.py
+++ b/solution.py
@@ -24,126 +24,6 @@
     for peer in peers:
         pl.semaphore_signal(barrier, inc=1, device_id=peer, device_id_type=MESH)
     pl.semaphore_wait(barrier, len(peers))
-
-
-def to_heads_kernel(n, *refs):
-    srcs, dsts = refs[:4], refs[4:8]
-    bounce, step_bounce, send, recv, local = refs[8:]
-    me = lax.axis_index("sp")
-    rows = srcs[0].shape[0]
-    width = dsts[0].shape[1]
-    peers = [lax.rem(me + i, n) for i in range(1, n)]
-    greet([{"sp": peer} for peer in peers])
-    copies = []
-    mine = pl.ds(pl.multiple_of(me * rows, rows), rows)
-    for i, peer in enumerate(peers):
-        for k in range(4):
-            if k < 3:
-                part = srcs[k].at[:, pl.ds(pl.multiple_of(peer * width, width), width)]
-                there = dsts[k].at[mine, :]
-            else:
-                part = srcs[k]
-                there = dsts[k].at[mine, :]
-            copy = pltpu.make_async_remote_copy(
-                src_ref=part,
-                dst_ref=there,
-                send_sem=send.at[i, k],
-                recv_sem=recv.at[i, k],
-                device_id={"sp": peer},
-                device_id_type=MESH,
-            )
-            copy.start()
-            copies.append(copy)
-    own = [srcs[k].at[:, pl.ds(pl.multiple_of(me * width, width), width)] for k in range(3)]
-    own.append(srcs[3])
-    slots = [bounce.at[k] for k in range(3)] + [step_bounce]
-    first = [pltpu.make_async_copy(own[k], slots[k], local.at[0, k]) for k in range(4)]
-    second = [
-        pltpu.make_async_copy(slots[k], dsts[k].at[mine, :], local.at[1, k]) for k in range(4)
-    ]
-    for k in range(4):
-        first[k].start()
-    for k in range(4):
-        first[k].wait()
-        second[k].start()
-    for k in range(4):
-        second[k].wait()
-    for copy in copies:
-        copy.wait()
-
-
-def to_heads(n, arrays, steps):
-    rows, full = arrays[0].shape
-    width = full // n
-    wide = jax.ShapeDtypeStruct((rows * n, width), arrays[0].dtype)
-    step_out = jax.ShapeDtypeStruct((rows * n, steps.shape[1]), steps.dtype)
-    anywhere = pl.BlockSpec(memory_space=pl.ANY)
-    return pl.pallas_call(
-        functools.partial(to_heads_kernel, n),
-        out_shape=(wide, wide, wide, step_out),
-        in_specs=[anywhere] * 4,
-        out_specs=(anywhere,) * 4,
-        scratch_shapes=[
-            pltpu.VMEM((3, rows, width), arrays[0].dtype),
-            pltpu.VMEM(steps.shape, steps.dtype),
-            pltpu.SemaphoreType.DMA((n - 1, 4)),
-            pltpu.SemaphoreType.DMA((n - 1, 4)),
-            pltpu.SemaphoreType.DMA((2, 4)),
-        ],
-        compiler_params=pltpu.CompilerParams(collective_id=1, has_side_effects=True),
-        name="to_heads",
-    )(*arrays, steps)
-
-
-def to_tokens_kernel(n, src, dst, bounce, send, recv, local):
-    me = lax.axis_index("sp")
-    rows = dst.shape[0]
-    width = src.shape[1]
-    peers = [lax.rem(me + i, n) for i in range(1, n)]
-    greet([{"sp": peer} for peer in peers])
-    there = dst.at[:, pl.ds(pl.multiple_of(me * width, width), width)]
-    copies = []
-    for i, peer in enumerate(peers):
-        copy = pltpu.make_async_remote_copy(
-            src_ref=src.at[pl.ds(pl.multiple_of(peer * rows, rows), rows), :],
-            dst_ref=there,
-            send_sem=send.at[i],
-            recv_sem=recv.at[i],
-            device_id={"sp": peer},
-            device_id_type=MESH,
-        )
-        copy.start()
-        copies.append(copy)
-    first = pltpu.make_async_copy(
-        src.at[pl.ds(pl.multiple_of(me * rows, rows), rows), :], bounce, local.at[0]
-    )
-    first.start()
-    first.wait()
-    second = pltpu.make_async_copy(bounce, there, local.at[1])
-    second.start()
-    second.wait()
-    for copy in copies:
-        copy.wait()
-
-
-def to_tokens(n, heads):
-    length, width = heads.shape
-    rows = length // n
-    anywhere = pl.BlockSpec(memory_space=pl.ANY)
-    return pl.pallas_call(
-        functools.partial(to_tokens_kernel, n),
-        out_shape=jax.ShapeDtypeStruct((rows, n * width), heads.dtype),
-        in_specs=[anywhere],
-        out_specs=anywhere,
-        scratch_shapes=[
-            pltpu.VMEM((rows, width), heads.dtype),
-            pltpu.SemaphoreType.DMA((n - 1,)),
-            pltpu.SemaphoreType.DMA((n - 1,)),
-            pltpu.SemaphoreType.DMA((2,)),
-        ],
-        compiler_params=pltpu.CompilerParams(collective_id=2, has_side_effects=True),
-        name="to_tokens",
-    )(heads)
 
 
 def plane_order(z, planes, s):
@@ -465,69 +345,180 @@
 
 
 def mixer_kernel(
-    x_ref, b_ref, c_ref, tx_ref, tb_ref, tc_ref, st_ref, stt_ref, rate_ref, ratet_ref,
-    o_ref, pad, reads, inside_ref, fade_f, fade_b, sums, carry,
+    n, taps_n, x_ref, b_ref, c_ref, z_ref, gain_ref, step_ref, edge_ref, tap_ref, out_ref,
+    taps, edges, halo, pad, reads, inside_ref, fade_f, fade_b, own_f, own_b, carry,
+    send_f, send_b, got_f, got_b, gated, cols, rows_t, squares,
+    tsend, trecv, esend, erecv, fsend, frecv, bsend, brecv, local,
 ):
-    length = x_ref.shape[0]
-    lanes = x_ref.shape[1]
-    blocks = length // BLOCK
-    per_group = st_ref.shape[2] // 2
-    taps = tx_ref.shape[0]
-    half = taps // 2
     f32, bf16 = jnp.float32, jnp.bfloat16
-    for k, ref in enumerate((x_ref, b_ref, c_ref)):
-        pad[k, 0:8, :] = jnp.zeros((8, lanes), f32)
-        pad[k, length + 8 : length + 16, :] = jnp.zeros((8, lanes), f32)
-        pad[k, 8 : length + 8, :] = ref[...].astype(f32)
-
-    def conv(k, taps_ref, base):
-        total = None
-        for j in range(taps):
-            term = pad[k, base + 8 - half + j : base + 8 - half + j + BLOCK, :] * taps_ref[j : j + 1, :]
-            total = term if total is None else total + term
-        return total * jax.nn.sigmoid(total)
-
-    def softplus(v):
-        return jnp.maximum(v, 0.0) + jnp.log(1.0 + jnp.exp(-jnp.abs(v)))
+    me = lax.axis_index("sp")
+    groups = own_f.shape[0]
+    lanes = x_ref.shape[1] // groups
+    per_group = lanes // HEAD_DIM
+    columns = 2 * per_group
+    half = taps_n // 2
+    wide = tap_ref.shape[1]
+    greet([{"sp": lax.rem(me + i, n)} for i in range(1, n)])
+    mine = pl.ds(pl.multiple_of(me * wide, wide), wide)
+
+    def tell(i):
+        return pltpu.make_async_remote_copy(
+            src_ref=tap_ref,
+            dst_ref=taps.at[:, mine],
+            send_sem=tsend.at[i],
+            recv_sem=trecv.at[i],
+            device_id={"sp": lax.rem(me + i, n)},
+            device_id_type=MESH,
+        )
+
+    def edge(way):
+        return pltpu.make_async_remote_copy(
+            src_ref=edge_ref.at[way],
+            dst_ref=edges.at[way],
+            send_sem=esend.at[way],
+            recv_sem=erecv.at[way],
+            device_id={"sp": me + 1 - 2 * way},
+            device_id_type=MESH,
+        )
+
+    has_next, has_last = me < n - 1, me > 0
+
+    @pl.when(has_next)
+    def _():
+        edge(0).start()
+
+    @pl.when(has_last)
+    def _():
+        edge(1).start()
+
+    for i in range(1, n):
+        tell(i).start()
+    keep = pltpu.make_async_copy(tap_ref, taps.at[:, mine], local.at[0])
+    keep.start()
+
+    @pl.when(jnp.logical_not(has_last))
+    def _():
+        halo[0] = jnp.zeros(halo.shape[1:], f32)
+        got_f[...] = jnp.zeros(got_f.shape, bf16)
+
+    @pl.when(jnp.logical_not(has_next))
+    def _():
+        halo[1] = jnp.zeros(halo.shape[1:], f32)
+        got_b[...] = jnp.zeros(got_b.shape, bf16)
 
     li = lax.broadcasted_iota(jnp.int32, (BLOCK, BLOCK), 0)
     si = lax.broadcasted_iota(jnp.int32, (BLOCK, BLOCK), 1)
-    at_or_after = li >= si
-    lower = jnp.where(at_or_after, 1.0, 0.0).astype(f32)
-    upper = jnp.where(si >= li, 1.0, 0.0).astype(f32)
+    lower = jnp.where(li >= si, 1.0, 0.0).astype(f32)
     lane_head = lax.broadcasted_iota(jnp.int32, (1, lanes), 1) // HEAD_DIM
 
-    def spread_heads(columns):
-        out = columns[0]
+    def spread_heads(values):
+        out = values[0]
         for h in range(1, per_group):
-            out = jnp.where(lane_head == h, columns[h], out)
+            out = jnp.where(lane_head == h, values[h], out)
         return jnp.broadcast_to(out, (out.shape[0], lanes))
 
-    for c in range(blocks):
-        base = c * BLOCK
-        rows = slice(base, base + BLOCK)
-        x = conv(0, tx_ref, base)
-        write = conv(1, tb_ref, base).astype(bf16)
-        read = conv(2, tc_ref, base).astype(bf16)
-        reads[rows, :] = read
-        dt = softplus(st_ref[0, rows, :])
-        dtt = softplus(stt_ref[0, :, rows])
-        a = dt * rate_ref[0]
-        at = dtt * ratet_ref[0]
-        inc = jnp.dot(lower, a, precision=highest, preferred_element_type=f32)
-        inct = jnp.dot(at, upper, precision=highest, preferred_element_type=f32)
-        exc = inc - a
-        exct = inct - at
+    v = step_ref[...]
+    dt = jnp.maximum(v, 0.0) + jnp.log(1.0 + jnp.exp(-jnp.abs(v)))
+    keep.wait()
+    for i in range(1, n):
+        tell(i).wait_recv()
+    rate = taps[3 * taps_n : 3 * taps_n + 1, 0 : v.shape[1]]
+    for i in range(1, n):
+        rate = rate + taps[3 * taps_n : 3 * taps_n + 1, i * wide : i * wide + v.shape[1]]
+    a = dt * rate
+    inc = jnp.dot(lower, a, precision=highest, preferred_element_type=f32)
+    exc = inc - a
+    for k, value in enumerate((inc, exc, dt)):
+        turned = value.T
+        for g in range(groups):
+            at = slice(g * columns, (g + 1) * columns)
+            cols[k, g, :, 0:columns] = value[:, at]
+            rows_t[k, g, 0:columns, :] = turned[at, :]
+
+    @pl.when(has_last)
+    def _():
+        edge(0).wait_recv()
+        halo[0] = edges[0].astype(f32)
+
+    @pl.when(has_next)
+    def _():
+        edge(1).wait_recv()
+        halo[1] = edges[1].astype(f32)
+
+    def pass_f(g):
+        return pltpu.make_async_remote_copy(
+            src_ref=send_f.at[g],
+            dst_ref=got_f.at[g],
+            send_sem=fsend.at[g],
+            recv_sem=frecv.at[g],
+            device_id={"sp": me + 1},
+            device_id_type=MESH,
+        )
+
+    def pass_b(g):
+        return pltpu.make_async_remote_copy(
+            src_ref=send_b.at[g],
+            dst_ref=got_b.at[g],
+            send_sem=bsend.at[g],
+            recv_sem=brecv.at[g],
+            device_id={"sp": me - 1},
+            device_id_type=MESH,
+        )
+
+    def local_part(g, unused):
+        at = pl.ds(pl.multiple_of(g * lanes, lanes), lanes)
+
+        def conv(k, ref):
+            pad[k, 8 - half : 8, :] = halo[0, k * half : (k + 1) * half, at]
+            pad[k, BLOCK + 8 : BLOCK + 8 + half, :] = halo[1, k * half : (k + 1) * half, at]
+            pad[k, 8 : BLOCK + 8, :] = ref[:, at].astype(f32)
+            total = None
+            for j in range(taps_n):
+                first = 8 - half + j
+                tap = taps[k * taps_n + j : k * taps_n + j + 1, at]
+                term = pad[k, first : first + BLOCK, :] * tap
+                total = term if total is None else total + term
+            return total * jax.nn.sigmoid(total)
+
+        x = conv(0, x_ref)
+        write = conv(1, b_ref).astype(bf16)
+        read = conv(2, c_ref).astype(bf16)
+        reads[g] = read
+        inc, exc, dt = (cols[k, g, :, 0:columns] for k in range(3))
+        inct, exct, dtt = (rows_t[k, g, 0:columns, :] for k in range(3))
         tot = inc[BLOCK - 1 : BLOCK, :]
-        scores = lax.dot_general(
-            read, write, (((1,), (1,)), ((), ())), preferred_element_type=f32
-        )
+        heads = range(per_group)
+        fwd = [inc[:, 2 * h : 2 * h + 1] for h in heads]
+        bwd = [exc[:, 2 * h + 1 : 2 * h + 2] for h in heads]
+        tot_f = [tot[:, 2 * h : 2 * h + 1] for h in heads]
+        tot_b = [tot[:, 2 * h + 1 : 2 * h + 2] for h in heads]
+        wf = spread_heads([dt[:, 2 * h : 2 * h + 1] * jnp.exp(fwd[h] - tot_f[h]) for h in heads])
+        wb = spread_heads([dt[:, 2 * h + 1 : 2 * h + 2] * jnp.exp(-bwd[h]) for h in heads])
+        both = jnp.concatenate([(x * wf).astype(bf16), (x * wb).astype(bf16)], axis=1)
+        sums = lax.dot_general(write, both, (((0,), (0,)), ((), ())), preferred_element_type=f32)
+        own_f[g] = sums[:, 0:lanes]
+        own_b[g] = sums[:, lanes : 2 * lanes]
+        carry[g, 0:1, :] = spread_heads([jnp.exp(-tot_f[h]) for h in heads])
+        carry[g, 1:2, :] = spread_heads([jnp.exp(-tot_b[h]) for h in heads])
+
+        @pl.when(jnp.logical_not(has_last))
+        def _():
+            send_f[g] = own_f[g].astype(bf16)
+            pass_f(g).start()
+
+        @pl.when(jnp.logical_not(has_next))
+        def _():
+            send_b[g] = own_b[g].astype(bf16)
+            pass_b(g).start()
+
+        fade_f[g] = spread_heads([jnp.exp(-fwd[h]) for h in heads])
+        fade_b[g] = spread_heads([jnp.exp(bwd[h] - tot_b[h]) for h in heads])
+        scores = lax.dot_general(read, write, (((1,), (1,)), ((), ())), preferred_element_type=f32)
         inside = None
-        xb = x.astype(bf16)
-        for h in range(per_group):
+        for h in heads:
             f, b = 2 * h, 2 * h + 1
             power = jnp.where(
-                at_or_after,
+                li >= si,
                 inct[f : f + 1, :] - inc[:, f : f + 1],
                 exc[:, b : b + 1] - exct[b : b + 1, :],
             )
@@ -537,104 +528,152 @@
             xh = jnp.where(lane_head == h, x, 0.0).astype(bf16)
             term = jnp.dot(weights, xh, preferred_element_type=f32)
             inside = term if inside is None else inside + term
-        inside_ref[rows, :] = inside
-        heads = range(per_group)
-        fwd = [inc[:, 2 * h : 2 * h + 1] for h in heads]
-        bwd = [exc[:, 2 * h + 1 : 2 * h + 2] for h in heads]
-        tot_f = [tot[:, 2 * h : 2 * h + 1] for h in heads]
-        tot_b = [tot[:, 2 * h + 1 : 2 * h + 2] for h in heads]
-        wf = spread_heads([dt[:, 2 * h : 2 * h + 1] * jnp.exp(fwd[h] - tot_f[h]) for h in heads])
-        wb = spread_heads([dt[:, 2 * h + 1 : 2 * h + 2] * jnp.exp(-bwd[h]) for h in heads])
-        fade_f[rows, :] = spread_heads([jnp.exp(-fwd[h]) for h in heads])
-        fade_b[rows, :] = spread_heads([jnp.exp(bwd[h] - tot_b[h]) for h in heads])
-        both = jnp.concatenate([(x * wf).astype(bf16), (x * wb).astype(bf16)], axis=1)
-        sums[c] = lax.dot_general(
-            write, both, (((0,), (0,)), ((), ())), preferred_element_type=f32
-        )
-        carry[c : c + 1, :] = jnp.concatenate(
-            [
-                spread_heads([jnp.exp(-tot_f[h]) for h in heads]),
-                spread_heads([jnp.exp(-tot_b[h]) for h in heads]),
-            ],
-            axis=1,
-        )
-
-    state = jnp.zeros((sums.shape[1], lanes), f32)
-    for c in range(blocks):
-        own = sums[c, :, 0:lanes]
-        sums[c, :, 0:lanes] = state
-        state = carry[c : c + 1, 0:lanes] * state + own
-    state = jnp.zeros((sums.shape[1], lanes), f32)
-    for c in reversed(range(blocks)):
-        own = sums[c, :, lanes : 2 * lanes]
-        sums[c, :, lanes : 2 * lanes] = state
-        state = carry[c : c + 1, lanes : 2 * lanes] * state + own
-    for c in range(blocks):
-        rows = slice(c * BLOCK, (c + 1) * BLOCK)
-        moved = jnp.dot(reads[rows, :], sums[c].astype(bf16), preferred_element_type=f32)
-        total = (
-            inside_ref[rows, :]
-            + moved[:, 0:lanes] * fade_f[rows, :]
-            + moved[:, lanes : 2 * lanes] * fade_b[rows, :]
-        )
-        o_ref[rows, :] = total.astype(o_ref.dtype)
-
-
-def mixer(signal, write, read, conv_x, conv_b, conv_c, steps, rates):
-    length, width = signal.shape
+        inside_ref[g] = inside
+        return unused
+
+    lax.fori_loop(0, groups, local_part, 0)
+
+    slack = 2
+    late_f = slack * jnp.maximum(2 * me - (n - 1), 0)
+    late_b = slack * jnp.maximum((n - 1) - 2 * me, 0)
+    late = jnp.maximum(late_f, late_b)
+    per_norm = groups // NORM_GROUPS
+    squares[...] = jnp.zeros(squares.shape, f32)
+
+    def relay(k, unused):
+        f, b, g = k - late_f, k - late_b, k - late
+
+        @pl.when(has_last & (f >= 0) & (f < groups))
+        def _():
+            pass_f(f).wait_recv()
+
+            @pl.when(has_next)
+            def _():
+                send_f[f] = (carry[f, 0:1, :] * got_f[f].astype(f32) + own_f[f]).astype(bf16)
+                pass_f(f).start()
+
+        @pl.when(has_next & (b >= 0) & (b < groups))
+        def _():
+            pass_b(b).wait_recv()
+
+            @pl.when(has_last)
+            def _():
+                send_b[b] = (carry[b, 1:2, :] * got_b[b].astype(f32) + own_b[b]).astype(bf16)
+                pass_b(b).start()
+
+        @pl.when((g >= 0) & (g < groups))
+        def _():
+            entering = jnp.concatenate([got_f[g], got_b[g]], axis=1)
+            moved = jnp.dot(reads[g], entering, preferred_element_type=f32)
+            total = (
+                inside_ref[g]
+                + moved[:, 0:lanes] * fade_f[g]
+                + moved[:, lanes : 2 * lanes] * fade_b[g]
+            )
+            at = pl.ds(pl.multiple_of(g * lanes, lanes), lanes)
+            gate = z_ref[:, at].astype(f32)
+            value = total.astype(bf16).astype(f32) * (gate * jax.nn.sigmoid(gate))
+            gated[g] = value
+            squares[g // per_norm] += jnp.sum(value * value, axis=1, keepdims=True)
+
+        return unused
+
+    lax.fori_loop(0, groups + slack * (n - 1), relay, 0)
+
+    def scale(g, unused):
+        at = pl.ds(pl.multiple_of(g * lanes, lanes), lanes)
+        mean = squares[g // per_norm] * (1.0 / (per_norm * lanes))
+        value = gated[g] * lax.rsqrt(mean + epsilon) * gain_ref[:, at]
+        out_ref[:, at] = value.astype(bf16)
+        return unused
+
+    lax.fori_loop(0, groups, scale, 0)
+
+    for i in range(1, n):
+        tell(i).wait_send()
+
+    @pl.when(has_next)
+    def _():
+        edge(0).wait_send()
+
+        def one(g, unused):
+            pass_f(g).wait_send()
+            return unused
+
+        lax.fori_loop(0, groups, one, 0)
+
+    @pl.when(has_last)
+    def _():
+        edge(1).wait_send()
+
+        def one(g, unused):
+            pass_b(g).wait_send()
+            return unused
+
+        lax.fori_loop(0, groups, one, 0)
+
+
+def mixer(n, signal, write, read, gate, gain, steps, conv_x, conv_b, conv_c, rates):
+    f32, bf16 = jnp.float32, jnp.bfloat16
+    tokens, width = signal.shape
     groups = write.shape[1] // STATE
     lanes = width // groups
-    columns = steps.shape[1] // groups
-    taps = conv_x.shape[0]
-    blocks = length // BLOCK
-    st = steps.astype(jnp.float32).reshape(length, groups, columns).transpose(1, 0, 2)
-    stt = st.transpose(0, 2, 1)
-    rate = rates.T.reshape(groups, 1, columns)
-    ratet = rates.T.reshape(groups, columns, 1)
-    wide = pl.BlockSpec((length, lanes), lambda g: (0, g))
-    state = pl.BlockSpec((length, STATE), lambda g: (0, g))
-    tap_x = pl.BlockSpec((taps, lanes), lambda g: (0, g))
-    tap_s = pl.BlockSpec((taps, STATE), lambda g: (0, g))
-
-    def whole(shape):
-        return pl.BlockSpec((1,) + shape, lambda g: (g, 0, 0))
-
-    f32 = jnp.float32
+    taps_n, wide = conv_x.shape
+    half = taps_n // 2
+    columns = steps.shape[1]
+    padded = max(columns, BLOCK)
+    own = rates.T.reshape(1, -1)
+    row = jnp.zeros((1, wide), f32)
+    row = lax.dynamic_update_slice(row, own, (0, lax.axis_index("sp") * own.shape[1]))
+    lines = 3 * taps_n + 1
+    spare = -lines % 8
+    taps = jnp.concatenate([conv_x, conv_b, conv_c, row, jnp.zeros((spare, wide), f32)], axis=0)
+    few = [signal, write, read]
+    blank = jnp.zeros((16 - 3 * half, width), bf16)
+    edges = jnp.stack(
+        [
+            jnp.concatenate([v[tokens - half :] for v in few] + [blank], axis=0),
+            jnp.concatenate([v[:half] for v in few] + [blank], axis=0),
+        ]
+    )
+    step = jnp.pad(steps.astype(f32), ((0, 0), (0, padded - columns)))
+    inside = pl.BlockSpec(memory_space=pltpu.VMEM)
+    dma = pltpu.SemaphoreType.DMA
+    tile = pltpu.VMEM((groups, tokens, lanes), f32)
+    state = pltpu.VMEM((groups, STATE, lanes), f32)
+    small = pltpu.VMEM((groups, STATE, lanes), bf16)
     return pl.pallas_call(
-        mixer_kernel,
-        grid=(groups,),
-        out_shape=jax.ShapeDtypeStruct((length, width), jnp.bfloat16),
-        in_specs=[
-            wide, state, state, tap_x, tap_s, tap_s,
-            whole((length, columns)), whole((columns, length)),
-            whole((1, columns)), whole((columns, 1)),
+        functools.partial(mixer_kernel, n, taps_n),
+        out_shape=jax.ShapeDtypeStruct((tokens, width), bf16),
+        in_specs=[inside] * 8,
+        out_specs=inside,
+        scratch_shapes=[
+            pltpu.VMEM((lines + spare, n * wide), f32),
+            pltpu.VMEM(edges.shape, bf16),
+            pltpu.VMEM(edges.shape, f32),
+            pltpu.VMEM((3, tokens + 16, lanes), f32),
+            pltpu.VMEM((groups, tokens, STATE), bf16),
+            tile, tile, tile, state, state,
+            pltpu.VMEM((groups, 8, lanes), f32),
+            small, small, small, small, tile,
+            pltpu.VMEM((3, groups, tokens, 8), f32),
+            pltpu.VMEM((3, groups, 8, tokens), f32),
+            pltpu.VMEM((NORM_GROUPS, tokens, 1), f32),
+            dma((n,)), dma((n,)), dma((2,)), dma((2,)),
+            dma((groups,)), dma((groups,)), dma((groups,)), dma((groups,)), dma((1,)),
         ],
-        out_specs=wide,
-        scratch_shapes=[
-            pltpu.VMEM((3, length + 16, lanes), f32),
-            pltpu.VMEM((length, STATE), jnp.bfloat16),
-            pltpu.VMEM((length, lanes), f32),
-            pltpu.VMEM((length, lanes), f32),
-            pltpu.VMEM((length, lanes), f32),
-            pltpu.VMEM((blocks, STATE, 2 * lanes), f32),
-            pltpu.VMEM((blocks, 2 * lanes), f32),
-        ],
-        compiler_params=pltpu.CompilerParams(vmem_limit_bytes=40 * 1024 * 1024),
+        compiler_params=pltpu.CompilerParams(
+            collective_id=1, has_side_effects=True, vmem_limit_bytes=40 * 1024 * 1024
+        ),
         cost_estimate=pl.CostEstimate(
-            flops=40 * 10**9, bytes_accessed=4 * length * width * 2, transcendentals=0
+            flops=40 * 10**9, bytes_accessed=4 * tokens * width * 2, transcendentals=0
         ),
         name="mixer",
-    )(signal, write, read, conv_x, conv_b, conv_c, st, stt, rate, ratet)
+    )(signal, write, read, gate, gain.reshape(1, width), step, edges, taps)
 
 
 def scale_rows(values, gains):
     return values * lax.rsqrt(jnp.mean(values * values, axis=-1, keepdims=True) + epsilon) * gains
-
-
-def group_scale(values, gains):
-    shaped = values.reshape(values.shape[:-1] + (NORM_GROUPS, values.shape[-1] // NORM_GROUPS))
-    shaped = shaped * lax.rsqrt(jnp.mean(shaped * shaped, axis=-1, keepdims=True) + epsilon)
-    return shaped.reshape(values.shape) * gains
 
 
 def gather_rows(weight, count):
@@ -656,18 +695,12 @@
     dp_count = lax.axis_size("dp")
     bf16, f32 = jnp.bfloat16, jnp.float32
     parts = gather_rows(out_weight, dp_count)
-    signal, write, read, steps = to_heads(
-        sp_count, (ssm_input[0], state_b[0], state_c[0]), step_raw[0]
+    mixed = mixer(
+        sp_count, ssm_input[0], state_b[0], state_c[0], gate_input[0], mix_gain, step_raw[0],
+        conv_x, conv_b, conv_c, decay_rate,
     )
-    columns = steps.shape[1] // sp_count
-    steps = lax.dynamic_slice_in_dim(steps, lax.axis_index("sp") * columns, columns, axis=1)
-    mixed_heads = mixer(signal, write, read, conv_x, conv_b, conv_c, steps, decay_rate)
-    mixed_tokens = to_tokens(sp_count, mixed_heads)
 
     token_count = residual_in.shape[1]
-    model_width = residual_in.shape[2]
-    gated = mixed_tokens.astype(f32) * jax.nn.silu(gate_input[0].astype(f32))
-    mixed = group_scale(gated, mix_gain).astype(bf16)
     depth = out_weight.shape[0]
     me = lax.axis_index("dp")
     stream = residual_in[0].astype(f32)

time: 216 us -> 259 us (1.20)
  waiting for transfers between devices: 0.01 us -> 39.6 us
  local copies, waits for them, and re-layouts: 5.67 us -> 10.8 us
  Pallas kernels: 190 us -> 194 us
  starting transfers between devices: 5.88 us -> 2.71 us
  other arithmetic: 6.9 us -> 3.81 us
    ppermute x3, waiting for transfers between devices: 0.01 us -> 39.6 us  [gather_rows(): parts[offset ^ step] = lax.ppermute(block, 'dp', pairs)]
    pallas_call x1, Pallas kernels: 126 us -> 138 us  [experts(): pl.pallas_call(functools.partial(experts_kernel, planes, inner, dp_count,...]
    pallas_call x3 -> x1, Pallas kernels: 63.7 us -> 56.2 us  [mixer(): pl.pallas_call(functools.partial(mixer_kernel, n, taps_n), out_shape=jax....]
    ppermute x3, starting transfers between devices: 5.88 us -> 2.71 us  [gather_rows(): parts[offset ^ step] = lax.ppermute(block, 'dp', pairs)]
    unnamed x32 -> x21, local copies, waits for them, and re-layouts: 3.25 us -> 5.71 us
  transfers between devices with their start and end apart: 3 -> 3, of which waited for: 0 -> 1; matrix products, arithmetic and copies ran while one was open for 6% -> 4% of each run, Pallas kernels for 30% -> 22%
where the time goes in v2:
time: 259 us; the launch traced here: 258 us
  Pallas kernels  194 us (75%)
  waiting for transfers between devices  39.6 us (15%)
  local copies, waits for them, and re-layouts  10.8 us (4%)
  matrix products  6.67 us (3%)
  other arithmetic  3.81 us (1%)
  starting transfers between devices  2.71 us (1%)
    pallas_call x1, Pallas kernels, experts(): pl.pallas_call(functools.partial(experts_kernel, planes, inner, dp_count,...  138 us
    pallas_call x1, Pallas kernels, mixer(): pl.pallas_call(functools.partial(mixer_kernel, n, taps_n), out_shape=jax....  56.2 us
    ppermute x3, waiting for transfers between devices, gather_rows(): parts[offset ^ step] = lax.ppermute(block, 'dp', pairs)  39.6 us
    dot_general x4, matrix products, per_device(): stream = stream + jnp.dot(piece, block, preferred_element_type=f32)  6.67 us
    unnamed x21, local copies, waits for them, and re-layouts  5.71 us
  transfers between devices with their start and end apart: 3, of which 1 were waited for; matrix products, arithmetic and copies ran while one was open for 4% of the time, Pallas kernels for 22%

profile of v2, /device:TPU:29, one launch (start us, length us, event | category | flops | bytes accessed | tf_op | source)
XLA Modules:
  0.0 258.2 jit_solution(6737118447743084896)
XLA Ops:
  0.0 0.2 collective-permute-start
  0.2 1.0 collective-permute-start.1
  1.2 0.8 copy.22
  2.0 0.8 copy.21
  2.9 0.2 dynamic_update_slice.3
  3.2 2.3 concatenate.14.tap_ref
  5.5 0.8 slice_bitcast_fusion.5
  6.3 0.8 slice_bitcast_fusion.3
  7.2 39.6 %collective-permute-done = bf16[512,2048]{1,0:T(8,128)(2,1)} collective-permute-done((bf16[512,2048]{1,0:T(8,128)(2,1)}, bf16[512,2048]{1,0:T(8,128)(2,1)}, u32[]{:S(2)}, u32[]{:S(2)}) %collective-permute-start) | collective-permute-done | bytes 2097184 | tf_op jit(solution)/shard_map/ppermute | solution.py:685
  46.8 1.5 collective-permute-start.2
  48.4 1.0 copy-done
  49.4 1.0 copy-done.1
  50.4 1.0 copy-done.2
  51.5 1.0 copy-done.3
  52.5 0.7 copy-done.4
  53.2 56.2 %mixer.1 = bf16[128,2048]{1,0:T(8,128)(2,1)S(1)} custom-call(bf16[128,2048]{1,0:T(8,128)(2,1)S(1)} %bitcast.39, bf16[128,2048]{1,0:T(8,128)(2,1)S(1)} %bitcast.40, bf16[128,2048]{1,0:T(8,128)(2,1)S(1)} %bitcast.41, bf16[128,2048]{1,0:T(8,128)(2,1)S(1)} %bitcast.42, f32[1,2048]{1,0:T(1,128)S(1)} %bitcast.43, f32[128,128]{1,0:T(8,128)S(1)} %pad_convert_fusion.step_ref, ...), custom_call_target="tpu_custom_call" | custom-call | flops 40000000000 | bytes 2097152 | tf_op jit(solution)/shard_map/mixer/pallas_call | solution.py:645
  109.5 0.6 pad_maximum_fusion.1.info_ref
  110.1 0.4 convolution_add_fusion.2
  110.6 2.0 fusion.3
  112.6 2.0 fusion
  114.7 2.1 multiply_reduce_fusion
  116.9 1.0 multiply_convert_fusion.x_ref
  117.8 138.2 %experts.1 = f32[128,2048]{1,0:T(8,128)} custom-call(bf16[128,2048]{1,0:T(8,128)(2,1)} %multiply_convert_fusion.x_ref, f32[8,128]{1,0:T(8,128)} %pad_maximum_fusion.1.info_ref, bf16[1,2048,1024]{2,1,0:T(8,128)(2,1)} %gate_hbm.1, bf16[1,2048,1024]{2,1,0:T(8,128)(2,1)} %up_hbm.1, bf16[1,1024,2048]{2,1,0:T(8,128)(2,1)} %down_hbm.1), custom_call_target="tpu_custom_call" | custom-call | flops 99999997952 | bytes 100000000 | tf_op jit(solution)/shard_map/experts/pallas_call | solution.py:321
  256.1 2.1 fusion.1
  (27 shorter events, 0.3 us)
Async XLA Ops:
  0.0 46.8 %collective-permute-start = (bf16[512,2048]{1,0:T(8,128)(2,1)}, bf16[512,2048]{1,0:T(8,128)(2,1)}, u32[]{:S(2)}, u32[]{:S(2)}) collective-permute-start(bf16[512,2048]{1,0:T(8,128)(2,1)} %param.29), channel_id=1, source_target_pairs={{0,2},{1,3},{2,0},{3,1},{4,6},{5,7},{6,4},{7,5},{8,10},{9,11},{10,... | collective-permute-start | bytes 6291464 | tf_op jit(solution)/shard_map/ppermute | solution.py:685
  0.2 110.4 %collective-permute-start.1 = (bf16[512,2048]{1,0:T(8,128)(2,1)}, bf16[512,2048]{1,0:T(8,128)(2,1)}, u32[]{:S(2)}, u32[]{:S(2)}) collective-permute-start(bf16[512,2048]{1,0:T(8,128)(2,1)} %param.29), channel_id=1, source_target_pairs={{0,1},{1,0},{2,3},{3,2},{4,5},{5,4},{6,7},{7,6},{8,9},{9,8},{10,11... | collective-permute-start | bytes 6291464 | tf_op jit(solution)/shard_map/ppermute | solution.py:685
  46.8 67.9 %collective-permute-start.2 = (bf16[512,2048]{1,0:T(8,128)(2,1)}, bf16[512,2048]{1,0:T(8,128)(2,1)}, u32[]{:S(2)}, u32[]{:S(2)}) collective-permute-start(bf16[512,2048]{1,0:T(8,128)(2,1)} %collective-permute-done), channel_id=1, source_target_pairs={{0,1},{1,0},{2,3},{3,2},{4,5},{5,4},{6,7},{7,6},{8,9},{9,8},{10,11... | collective-permute-start | bytes 6291464 | tf_op jit(solution)/shard_map/ppermute | solution.py:685
  48.4 1.0 copy-start
  49.4 1.0 copy-start.1
  50.4 1.0 copy-start.2
  51.5 1.0 copy-start.3
  52.5 0.7 copy-start.4
  53.2 56.3 %copy-start.8 = (s32[1,128,4]{1,2,0:T(4,128)S(1)}, s32[1,128,4]{1,2,0:T(4,128)}, u32[]{:S(2)}) copy-start(s32[1,128,4]{1,2,0:T(4,128)} %param.31) | copy-start | bytes 6148
  53.2 56.3 %copy-start.9 = (f32[1,128,4]{1,2,0:T(4,128)S(1)}, f32[1,128,4]{1,2,0:T(4,128)}, u32[]{:S(2)}) copy-start(f32[1,128,4]{1,2,0:T(4,128)} %param.32) | copy-start | bytes 6148
  53.2 56.9 %copy-start.5 = (bf16[512,2048]{1,0:T(8,128)(2,1)S(1)}, bf16[512,2048]{1,0:T(8,128)(2,1)}, u32[]{:S(2)}) copy-start(bf16[512,2048]{1,0:T(8,128)(2,1)} %param.29) | copy-start | bytes 6291460
  53.2 56.9 %copy-start.6 = (bf16[1,128,2048]{2,1,0:T(8,128)(2,1)S(1)}, bf16[1,128,2048]{2,1,0:T(8,128)(2,1)}, u32[]{:S(2)}) copy-start(bf16[1,128,2048]{2,1,0:T(8,128)(2,1)} %param.18) | copy-start | bytes 1572868
  114.7 2.2 copy-start.7

commit v3 on v2

--- a/solution.py
+++ b/solution.py
@@ -344,64 +344,159 @@
     )(tokens_in, info, gate_w, up_w, down_w)
 
 
+def lowest(offset):
+    return offset & -offset
+
+
 def mixer_kernel(
-    n, taps_n, x_ref, b_ref, c_ref, z_ref, gain_ref, step_ref, edge_ref, tap_ref, out_ref,
-    taps, edges, halo, pad, reads, inside_ref, fade_f, fade_b, own_f, own_b, carry,
-    send_f, send_b, got_f, got_b, gated, cols, rows_t, squares,
-    tsend, trecv, esend, erecv, fsend, frecv, bsend, brecv, local,
+    n, inner, dp_count, x_hbm, b_hbm, c_hbm, z_hbm, r_hbm, w_hbm, step_ref, tx_ref, tb_ref, tc_ref,
+    rate_ref, gain_ref, ffn_gain_ref, stream_ref, ffn_ref,
+    ins, gate_v, res_v, w_all, steps, taps, rates, halo_in, halo, pad, reads, inside_ref,
+    fade_f, fade_b, own_f, own_b, carry, send_f, send_b, got_f, got_b, ybuf, ytok, gated, mixed,
+    cols, rows_t, squares,
+    in_s, in_r, step_s, step_r, tap_s, tap_r, rate_s, rate_r, halo_s, halo_r,
+    f_s, f_r, b_s, b_r, y_s, y_r, w_s, w_r, own_in, local,
 ):
     f32, bf16 = jnp.float32, jnp.bfloat16
-    me = lax.axis_index("sp")
-    groups = own_f.shape[0]
-    lanes = x_ref.shape[1] // groups
+    sp, dp = lax.axis_index("sp"), lax.axis_index("dp")
+    z, x = sp // inner, lax.rem(sp, inner)
+    planes = n // inner
+    tokens, width = stream_ref.shape
+    span = ins.shape[3]
+    locals_n = own_f.shape[0]
+    lanes = span // locals_n
+    groups = locals_n * inner
     per_group = lanes // HEAD_DIM
     columns = 2 * per_group
+    taps_n, wide = tx_ref.shape
     half = taps_n // 2
-    wide = tap_ref.shape[1]
-    greet([{"sp": lax.rem(me + i, n)} for i in range(1, n)])
-    mine = pl.ds(pl.multiple_of(me * wide, wide), wide)
-
-    def tell(i):
+    depth = w_hbm.shape[0]
+    piece = min(depth, 128)
+    pieces = depth // piece
+    bits = [1 << i for i in range(dp_count.bit_length() - 1)]
+    flows = (x_hbm, b_hbm, c_hbm)
+    tap_refs = (tx_ref, tb_ref, tc_ref)
+
+    def mate(bit):
+        return dp + bit * (1 - 2 * lax.rem(dp // bit, 2))
+
+    greet([{"sp": lax.rem(sp + i, n)} for i in range(1, n)] + [{"dp": mate(b)} for b in bits])
+
+    def remote(src, dst, send, recv, where):
         return pltpu.make_async_remote_copy(
-            src_ref=tap_ref,
-            dst_ref=taps.at[:, mine],
-            send_sem=tsend.at[i],
-            recv_sem=trecv.at[i],
-            device_id={"sp": lax.rem(me + i, n)},
-            device_id_type=MESH,
-        )
-
-    def edge(way):
-        return pltpu.make_async_remote_copy(
-            src_ref=edge_ref.at[way],
-            dst_ref=edges.at[way],
-            send_sem=esend.at[way],
-            recv_sem=erecv.at[way],
-            device_id={"sp": me + 1 - 2 * way},
-            device_id_type=MESH,
-        )
-
-    has_next, has_last = me < n - 1, me > 0
-
-    @pl.when(has_next)
-    def _():
-        edge(0).start()
-
-    @pl.when(has_last)
-    def _():
-        edge(1).start()
-
+            src_ref=src, dst_ref=dst, send_sem=send, recv_sem=recv,
+            device_id=where, device_id_type=MESH,
+        )
+
+    def spot(start, size):
+        return pl.ds(pl.multiple_of(start, size), size)
+
+    def give_step(i):
+        return remote(
+            step_ref, steps.at[x], step_s.at[i], step_r.at[i],
+            {"sp": z * inner + lax.rem(x + i, inner)},
+        )
+
+    mine = spot(sp * wide, wide)
+
+    def give_tap(k, i):
+        return remote(
+            tap_refs[k], taps.at[k, 0:taps_n, mine], tap_s.at[k, i], tap_r.at[k, i],
+            {"sp": lax.rem(sp + i, n)},
+        )
+
+    def give_rate(i):
+        return remote(
+            rate_ref, rates.at[sp], rate_s.at[i], rate_r.at[i], {"sp": lax.rem(sp + i, n)}
+        )
+
+    def give_halo(way, k, to):
+        first = 0 if way else tokens - 8
+        return remote(
+            flows[k].at[first : first + 8, to * span : (to + 1) * span],
+            halo_in.at[way, k], halo_s.at[way, k, to], halo_r.at[way, k],
+            {"sp": (z + 1 - 2 * way) * inner + to},
+        )
+
+    def give_in(k, q, i):
+        peer = lax.rem(x + i, inner)
+        return remote(
+            flows[k].at[:, spot(peer * span + q * lanes, lanes)],
+            ins.at[k, x, :, spot(q * lanes, lanes)],
+            in_s.at[k, q, i], in_r.at[k, q, i], {"sp": z * inner + peer},
+        )
+
+    def give_weight(offset, bit, c):
+        rows = slice(c * piece, (c + 1) * piece)
+        src = w_hbm.at[rows] if offset == 0 else w_all.at[offset, rows]
+        return remote(
+            src, w_all.at[offset + bit, rows],
+            w_s.at[offset, bits.index(bit), c], w_r.at[offset + bit, c], {"dp": mate(bit)},
+        )
+
+    has_above, has_below = z < planes - 1, z > 0
+    sends_up = has_above & (x == inner - 1)
+    sends_down = has_below & (x == 0)
+
+    for i in range(1, inner):
+        give_step(i).start()
     for i in range(1, n):
-        tell(i).start()
-    keep = pltpu.make_async_copy(tap_ref, taps.at[:, mine], local.at[0])
-    keep.start()
-
-    @pl.when(jnp.logical_not(has_last))
+        for k in range(3):
+            give_tap(k, i).start()
+        give_rate(i).start()
+
+    @pl.when(sends_up)
+    def _():
+        for k in range(3):
+            for to in range(inner):
+                give_halo(0, k, to).start()
+
+    @pl.when(sends_down)
+    def _():
+        for k in range(3):
+            for to in range(inner):
+                give_halo(1, k, to).start()
+
+    def begin(q, unused):
+        for k in range(3):
+            for i in range(1, inner):
+                give_in(k, q, i).start()
+        return unused
+
+    lax.fori_loop(0, locals_n, begin, 0)
+    owned = [
+        pltpu.make_async_copy(
+            flows[k].at[:, spot(x * span, span)], ins.at[k, x], own_in.at[k]
+        )
+        for k in range(3)
+    ]
+    for copy in owned:
+        copy.start()
+    for bit in reversed(bits):
+        for c in range(pieces):
+            give_weight(0, bit, c).start()
+    keeps = [
+        pltpu.make_async_copy(tap_refs[k], taps.at[k, 0:taps_n, mine], local.at[k])
+        for k in range(3)
+    ]
+    keeps.append(pltpu.make_async_copy(rate_ref, rates.at[sp], local.at[3]))
+    keeps.append(pltpu.make_async_copy(step_ref, steps.at[x], local.at[4]))
+    for copy in keeps:
+        copy.start()
+    late_loads = [
+        pltpu.make_async_copy(z_hbm, gate_v, local.at[5]),
+        pltpu.make_async_copy(r_hbm, res_v, local.at[6]),
+        pltpu.make_async_copy(w_hbm, w_all.at[0], local.at[7]),
+    ]
+    for copy in late_loads:
+        copy.start()
+
+    @pl.when(jnp.logical_not(has_below))
     def _():
         halo[0] = jnp.zeros(halo.shape[1:], f32)
         got_f[...] = jnp.zeros(got_f.shape, bf16)
 
-    @pl.when(jnp.logical_not(has_next))
+    @pl.when(jnp.logical_not(has_above))
     def _():
         halo[1] = jnp.zeros(halo.shape[1:], f32)
         got_b[...] = jnp.zeros(got_b.shape, bf16)
@@ -409,7 +504,8 @@
     li = lax.broadcasted_iota(jnp.int32, (BLOCK, BLOCK), 0)
     si = lax.broadcasted_iota(jnp.int32, (BLOCK, BLOCK), 1)
     lower = jnp.where(li >= si, 1.0, 0.0).astype(f32)
-    lane_head = lax.broadcasted_iota(jnp.int32, (1, lanes), 1) // HEAD_DIM
+    lane = lax.broadcasted_iota(jnp.int32, (1, lanes), 1)
+    lane_head = lane // HEAD_DIM
 
     def spread_heads(values):
         out = values[0]
@@ -417,274 +513,403 @@
             out = jnp.where(lane_head == h, values[h], out)
         return jnp.broadcast_to(out, (out.shape[0], lanes))
 
-    v = step_ref[...]
-    dt = jnp.maximum(v, 0.0) + jnp.log(1.0 + jnp.exp(-jnp.abs(v)))
-    keep.wait()
+    for copy in keeps:
+        copy.wait()
     for i in range(1, n):
-        tell(i).wait_recv()
-    rate = taps[3 * taps_n : 3 * taps_n + 1, 0 : v.shape[1]]
+        give_rate(i).wait_recv()
+    step_columns = step_ref.shape[1]
+    window = step_columns // inner
+    held = rate_ref.shape[1]
+    rate = jnp.zeros((1, BLOCK), f32)
+    row_lane = lax.broadcasted_iota(jnp.int32, (1, BLOCK), 1)
+    for t in range(planes):
+        pair = rates[x * planes + t]
+        for h in range(held):
+            for d in range(2):
+                rate = jnp.where(
+                    row_lane == 2 * (t * held + h) + d, pair[d : d + 1, h : h + 1], rate
+                )
+    choose_row = lax.broadcasted_iota(jnp.int32, (step_columns, BLOCK), 0)
+    choose_col = lax.broadcasted_iota(jnp.int32, (step_columns, BLOCK), 1)
+    choose = jnp.where((choose_row == x * window + choose_col) & (choose_col < window), 1.0, 0.0)
+    choose = choose.astype(bf16)
+    for i in range(1, inner):
+        give_step(i).wait_recv()
+    for i in range(inner):
+        v = jnp.dot(steps[i], choose, preferred_element_type=f32)
+        dt = jnp.maximum(v, 0.0) + jnp.log(1.0 + jnp.exp(-jnp.abs(v)))
+        a = dt * rate
+        inc = jnp.dot(lower, a, precision=highest, preferred_element_type=f32)
+        exc = inc - a
+        for k, value in enumerate((inc, exc, dt)):
+            turned = value.T
+            for q in range(locals_n):
+                at = slice(q * columns, (q + 1) * columns)
+                cols[k, i, q, :, 0:columns] = value[:, at]
+                rows_t[k, i, q, 0:columns, :] = turned[at, :]
+
     for i in range(1, n):
-        rate = rate + taps[3 * taps_n : 3 * taps_n + 1, i * wide : i * wide + v.shape[1]]
-    a = dt * rate
-    inc = jnp.dot(lower, a, precision=highest, preferred_element_type=f32)
-    exc = inc - a
-    for k, value in enumerate((inc, exc, dt)):
-        turned = value.T
-        for g in range(groups):
-            at = slice(g * columns, (g + 1) * columns)
-            cols[k, g, :, 0:columns] = value[:, at]
-            rows_t[k, g, 0:columns, :] = turned[at, :]
-
-    @pl.when(has_last)
-    def _():
-        edge(0).wait_recv()
-        halo[0] = edges[0].astype(f32)
-
-    @pl.when(has_next)
-    def _():
-        edge(1).wait_recv()
-        halo[1] = edges[1].astype(f32)
-
-    def pass_f(g):
-        return pltpu.make_async_remote_copy(
-            src_ref=send_f.at[g],
-            dst_ref=got_f.at[g],
-            send_sem=fsend.at[g],
-            recv_sem=frecv.at[g],
-            device_id={"sp": me + 1},
-            device_id_type=MESH,
-        )
-
-    def pass_b(g):
-        return pltpu.make_async_remote_copy(
-            src_ref=send_b.at[g],
-            dst_ref=got_b.at[g],
-            send_sem=bsend.at[g],
-            recv_sem=brecv.at[g],
-            device_id={"sp": me - 1},
-            device_id_type=MESH,
-        )
-
-    def local_part(g, unused):
-        at = pl.ds(pl.multiple_of(g * lanes, lanes), lanes)
-
-        def conv(k, ref):
-            pad[k, 8 - half : 8, :] = halo[0, k * half : (k + 1) * half, at]
-            pad[k, BLOCK + 8 : BLOCK + 8 + half, :] = halo[1, k * half : (k + 1) * half, at]
-            pad[k, 8 : BLOCK + 8, :] = ref[:, at].astype(f32)
+        for k in range(3):
+            give_tap(k, i).wait_recv()
+
+    @pl.when(has_below)
+    def _():
+        for k in range(3):
+            give_halo(0, k, 0).wait_recv()
+        halo[0] = halo_in[0].astype(f32)
+
+    @pl.when(has_above)
+    def _():
+        for k in range(3):
+            give_halo(1, k, 0).wait_recv()
+        halo[1] = halo_in[1].astype(f32)
+
+    for copy in owned:
+        copy.wait()
+
+    def pass_f(q):
+        return remote(
+            send_f.at[q], got_f.at[q], f_s.at[q], f_r.at[q], {"sp": sp + inner}
+        )
+
+    def pass_b(q):
+        return remote(
+            send_b.at[q], got_b.at[q], b_s.at[q], b_r.at[q], {"sp": sp - inner}
+        )
+
+    def onward_f(q, value):
+        for i in range(inner):
+            value = carry[q, i, 0:1, :] * value + own_f[q, i]
+        send_f[q] = value.astype(bf16)
+        pass_f(q).start()
+
+    def onward_b(q, value):
+        for i in reversed(range(inner)):
+            value = carry[q, i, 1:2, :] * value + own_b[q, i]
+        send_b[q] = value.astype(bf16)
+        pass_b(q).start()
+
+    def local_part(q):
+        at = spot(q * lanes, lanes)
+        wide_at = spot(x * span + q * lanes, lanes)
+        length = inner * tokens
+        for k in range(3):
+            pad[k, 8 - half : 8, :] = halo[0, k, 8 - half : 8, at]
+            pad[k, length + 8 : length + 8 + half, :] = halo[1, k, 0:half, at]
+            for i in range(inner):
+                pad[k, i * tokens + 8 : (i + 1) * tokens + 8, :] = ins[k, i, :, at].astype(f32)
+
+        def conv(k, i):
             total = None
             for j in range(taps_n):
-                first = 8 - half + j
-                tap = taps[k * taps_n + j : k * taps_n + j + 1, at]
-                term = pad[k, first : first + BLOCK, :] * tap
+                first = i * tokens + 8 - half + j
+                term = pad[k, first : first + tokens, :] * taps[k, j : j + 1, wide_at]
                 total = term if total is None else total + term
             return total * jax.nn.sigmoid(total)
 
-        x = conv(0, x_ref)
-        write = conv(1, b_ref).astype(bf16)
-        read = conv(2, c_ref).astype(bf16)
-        reads[g] = read
-        inc, exc, dt = (cols[k, g, :, 0:columns] for k in range(3))
-        inct, exct, dtt = (rows_t[k, g, 0:columns, :] for k in range(3))
-        tot = inc[BLOCK - 1 : BLOCK, :]
-        heads = range(per_group)
-        fwd = [inc[:, 2 * h : 2 * h + 1] for h in heads]
-        bwd = [exc[:, 2 * h + 1 : 2 * h + 2] for h in heads]
-        tot_f = [tot[:, 2 * h : 2 * h + 1] for h in heads]
-        tot_b = [tot[:, 2 * h + 1 : 2 * h + 2] for h in heads]
-        wf = spread_heads([dt[:, 2 * h : 2 * h + 1] * jnp.exp(fwd[h] - tot_f[h]) for h in heads])
-        wb = spread_heads([dt[:, 2 * h + 1 : 2 * h + 2] * jnp.exp(-bwd[h]) for h in heads])
-        both = jnp.concatenate([(x * wf).astype(bf16), (x * wb).astype(bf16)], axis=1)
-        sums = lax.dot_general(write, both, (((0,), (0,)), ((), ())), preferred_element_type=f32)
-        own_f[g] = sums[:, 0:lanes]
-        own_b[g] = sums[:, lanes : 2 * lanes]
-        carry[g, 0:1, :] = spread_heads([jnp.exp(-tot_f[h]) for h in heads])
-        carry[g, 1:2, :] = spread_heads([jnp.exp(-tot_b[h]) for h in heads])
-
-        @pl.when(jnp.logical_not(has_last))
-        def _():
-            send_f[g] = own_f[g].astype(bf16)
-            pass_f(g).start()
-
-        @pl.when(jnp.logical_not(has_next))
-        def _():
-            send_b[g] = own_b[g].astype(bf16)
-            pass_b(g).start()
-
-        fade_f[g] = spread_heads([jnp.exp(-fwd[h]) for h in heads])
-        fade_b[g] = spread_heads([jnp.exp(bwd[h] - tot_b[h]) for h in heads])
-        scores = lax.dot_general(read, write, (((1,), (1,)), ((), ())), preferred_element_type=f32)
-        inside = None
-        for h in heads:
-            f, b = 2 * h, 2 * h + 1
-            power = jnp.where(
-                li >= si,
-                inct[f : f + 1, :] - inc[:, f : f + 1],
-                exc[:, b : b + 1] - exct[b : b + 1, :],
+        for i in range(inner):
+            xs = conv(0, i)
+            write = conv(1, i).astype(bf16)
+            read = conv(2, i).astype(bf16)
+            reads[q, i] = read
+            inc, exc, dt = (cols[k, i, q, :, 0:columns] for k in range(3))
+            inct, exct, dtt = (rows_t[k, i, q, 0:columns, :] for k in range(3))
+            tot = inc[BLOCK - 1 : BLOCK, :]
+            heads = range(per_group)
+            fwd = [inc[:, 2 * h : 2 * h + 1] for h in heads]
+            bwd = [exc[:, 2 * h + 1 : 2 * h + 2] for h in heads]
+            tot_f = [tot[:, 2 * h : 2 * h + 1] for h in heads]
+            tot_b = [tot[:, 2 * h + 1 : 2 * h + 2] for h in heads]
+            wf = spread_heads(
+                [dt[:, 2 * h : 2 * h + 1] * jnp.exp(fwd[h] - tot_f[h]) for h in heads]
             )
-            df, db = dtt[f : f + 1, :], dtt[b : b + 1, :]
-            scale = jnp.where(li > si, df, jnp.where(li == si, df + db, db))
-            weights = (scores * jnp.exp(power) * scale).astype(bf16)
-            xh = jnp.where(lane_head == h, x, 0.0).astype(bf16)
-            term = jnp.dot(weights, xh, preferred_element_type=f32)
-            inside = term if inside is None else inside + term
-        inside_ref[g] = inside
+            wb = spread_heads([dt[:, 2 * h + 1 : 2 * h + 2] * jnp.exp(-bwd[h]) for h in heads])
+            both = jnp.concatenate([(xs * wf).astype(bf16), (xs * wb).astype(bf16)], axis=1)
+            sums = lax.dot_general(
+                write, both, (((0,), (0,)), ((), ())), preferred_element_type=f32
+            )
+            own_f[q, i] = sums[:, 0:lanes]
+            own_b[q, i] = sums[:, lanes : 2 * lanes]
+            carry[q, i, 0:1, :] = spread_heads([jnp.exp(-tot_f[h]) for h in heads])
+            carry[q, i, 1:2, :] = spread_heads([jnp.exp(-tot_b[h]) for h in heads])
+            fade_f[q, i] = spread_heads([jnp.exp(-fwd[h]) for h in heads])
+            fade_b[q, i] = spread_heads([jnp.exp(bwd[h] - tot_b[h]) for h in heads])
+            scores = lax.dot_general(
+                read, write, (((1,), (1,)), ((), ())), preferred_element_type=f32
+            )
+            inside = None
+            for h in heads:
+                f, b = 2 * h, 2 * h + 1
+                power = jnp.where(
+                    li >= si,
+                    inct[f : f + 1, :] - inc[:, f : f + 1],
+                    exc[:, b : b + 1] - exct[b : b + 1, :],
+                )
+                df, db = dtt[f : f + 1, :], dtt[b : b + 1, :]
+                scale = jnp.where(li > si, df, jnp.where(li == si, df + db, db))
+                weights = (scores * jnp.exp(power) * scale).astype(bf16)
+                xh = jnp.where(lane_head == h, xs, 0.0).astype(bf16)
+                term = jnp.dot(weights, xh, preferred_element_type=f32)
+                inside = term if inside is None else inside + term
+            inside_ref[q, i] = inside
+
+        @pl.when(has_above & jnp.logical_not(has_below))
+        def _():
+            onward_f(q, jnp.zeros((STATE, lanes), f32))
+
+        @pl.when(has_below & jnp.logical_not(has_above))
+        def _():
+            onward_b(q, jnp.zeros((STATE, lanes), f32))
+
+    def give_y(q, to):
+        i = lax.rem(to - x + inner, inner)
+        return remote(
+            ybuf.at[q, to], ytok.at[:, spot((x * locals_n + q) * lanes, lanes)],
+            y_s.at[i, q], y_r.at[i, q], {"sp": z * inner + to},
+        )
+
+    def finish(q):
+        enter_f, enter_b = [], [None] * inner
+        value = got_f[q].astype(f32)
+        for i in range(inner):
+            enter_f.append(value.astype(bf16))
+            if i < inner - 1:
+                value = carry[q, i, 0:1, :] * value + own_f[q, i]
+        value = got_b[q].astype(f32)
+        for i in reversed(range(inner)):
+            enter_b[i] = value.astype(bf16)
+            if i > 0:
+                value = carry[q, i, 1:2, :] * value + own_b[q, i]
+        for i in range(inner):
+            entering = jnp.concatenate([enter_f[i], enter_b[i]], axis=1)
+            moved = jnp.dot(reads[q, i], entering, preferred_element_type=f32)
+            total = (
+                inside_ref[q, i]
+                + moved[:, 0:lanes] * fade_f[q, i]
+                + moved[:, lanes : 2 * lanes] * fade_b[q, i]
+            )
+            ybuf[q, i] = total.astype(bf16)
+
+            @pl.when(x == i)
+            def _():
+                ytok[:, spot((x * locals_n + q) * lanes, lanes)] = ybuf[q, i]
+
+            @pl.when(x != i)
+            def _():
+                give_y(q, i).start()
+
+    late_f = (3 * z + 1) // 2
+    late_b = (3 * (planes - 1 - z) + 1) // 2
+    late = jnp.maximum(late_f, late_b)
+
+    def turn(t, unused):
+        f, b, g = t - late_f, t - late_b, t - late
+
+        @pl.when(t < locals_n)
+        def _():
+            for k in range(3):
+                for i in range(1, inner):
+                    give_in(k, t, i).wait_recv()
+            local_part(t)
+
+        @pl.when(has_below & (f >= 0) & (f < locals_n))
+        def _():
+            pass_f(f).wait_recv()
+
+            @pl.when(has_above)
+            def _():
+                onward_f(f, got_f[f].astype(f32))
+
+        @pl.when(has_above & (b >= 0) & (b < locals_n))
+        def _():
+            pass_b(b).wait_recv()
+
+            @pl.when(has_below)
+            def _():
+                onward_b(b, got_b[b].astype(f32))
+
+        @pl.when((g >= 0) & (g < locals_n))
+        def _():
+            finish(g)
+
         return unused
 
-    lax.fori_loop(0, groups, local_part, 0)
-
-    slack = 2
-    late_f = slack * jnp.maximum(2 * me - (n - 1), 0)
-    late_b = slack * jnp.maximum((n - 1) - 2 * me, 0)
-    late = jnp.maximum(late_f, late_b)
+    lax.fori_loop(0, locals_n + (3 * (planes - 1) + 1) // 2, turn, 0)
+
     per_norm = groups // NORM_GROUPS
     squares[...] = jnp.zeros(squares.shape, f32)
-
-    def relay(k, unused):
-        f, b, g = k - late_f, k - late_b, k - late
-
-        @pl.when(has_last & (f >= 0) & (f < groups))
-        def _():
-            pass_f(f).wait_recv()
-
-            @pl.when(has_next)
-            def _():
-                send_f[f] = (carry[f, 0:1, :] * got_f[f].astype(f32) + own_f[f]).astype(bf16)
-                pass_f(f).start()
-
-        @pl.when(has_next & (b >= 0) & (b < groups))
-        def _():
-            pass_b(b).wait_recv()
-
-            @pl.when(has_last)
-            def _():
-                send_b[b] = (carry[b, 1:2, :] * got_b[b].astype(f32) + own_b[b]).astype(bf16)
-                pass_b(b).start()
-
-        @pl.when((g >= 0) & (g < groups))
-        def _():
-            entering = jnp.concatenate([got_f[g], got_b[g]], axis=1)
-            moved = jnp.dot(reads[g], entering, preferred_element_type=f32)
-            total = (
-                inside_ref[g]
-                + moved[:, 0:lanes] * fade_f[g]
-                + moved[:, lanes : 2 * lanes] * fade_b[g]
-            )
-            at = pl.ds(pl.multiple_of(g * lanes, lanes), lanes)
-            gate = z_ref[:, at].astype(f32)
-            value = total.astype(bf16).astype(f32) * (gate * jax.nn.sigmoid(gate))
-            gated[g] = value
-            squares[g // per_norm] += jnp.sum(value * value, axis=1, keepdims=True)
-
+    for copy in late_loads:
+        copy.wait()
+
+    def gate_group(g, unused):
+        owner, q = g // locals_n, lax.rem(g, locals_n)
+
+        @pl.when(owner != x)
+        def _():
+            i = lax.rem(x - owner + inner, inner)
+            remote(
+                ybuf.at[q, 0], ytok.at[:, spot(g * lanes, lanes)],
+                y_s.at[i, q], y_r.at[i, q], {"sp": z * inner + owner},
+            ).wait_recv()
+
+        at = spot(g * lanes, lanes)
+        gate = gate_v[:, at].astype(f32)
+        value = ytok[:, at].astype(f32) * (gate * jax.nn.sigmoid(gate))
+        gated[g] = value
+        squares[g // per_norm] += jnp.sum(value * value, axis=1, keepdims=True)
         return unused
 
-    lax.fori_loop(0, groups + slack * (n - 1), relay, 0)
+    lax.fori_loop(0, groups, gate_group, 0)
 
     def scale(g, unused):
-        at = pl.ds(pl.multiple_of(g * lanes, lanes), lanes)
+        at = spot(g * lanes, lanes)
         mean = squares[g // per_norm] * (1.0 / (per_norm * lanes))
         value = gated[g] * lax.rsqrt(mean + epsilon) * gain_ref[:, at]
-        out_ref[:, at] = value.astype(bf16)
+        mixed[:, at] = value.astype(bf16)
         return unused
 
     lax.fori_loop(0, groups, scale, 0)
 
+    stream_ref[...] = res_v[...].astype(f32)
+    order = sorted(range(1, dp_count), key=lambda o: (-lowest(o), o))
+    for offset in [0] + order:
+        if offset:
+            for c in range(pieces):
+                give_weight(offset - lowest(offset), lowest(offset), c).wait_recv()
+                for bit in bits:
+                    if bit < lowest(offset):
+                        give_weight(offset, bit, c).start()
+        block = dp
+        for bit in bits:
+            if offset & bit:
+                block = block + bit * (1 - 2 * lax.rem(dp // bit, 2))
+        part = mixed[:, spot(block * depth, depth)]
+
+        def project(t, unused):
+            at = spot(t * 512, 512)
+            stream_ref[:, at] += jnp.dot(
+                part, w_all[offset, :, at], preferred_element_type=f32
+            )
+            return unused
+
+        lax.fori_loop(0, width // 512, project, 0)
+    total = jnp.zeros((tokens, 1), f32)
+    for at in range(0, width, 512):
+        value = stream_ref[:, at : at + 512]
+        total = total + jnp.sum(value * value, axis=1, keepdims=True)
+    root = lax.rsqrt(total * (1.0 / width) + epsilon)
+    for at in range(0, width, 512):
+        value = stream_ref[:, at : at + 512] * root * ffn_gain_ref[:, at : at + 512]
+        ffn_ref[:, at : at + 512] = value.astype(bf16)
+
+    for i in range(1, inner):
+        give_step(i).wait_send()
     for i in range(1, n):
-        tell(i).wait_send()
-
-    @pl.when(has_next)
-    def _():
-        edge(0).wait_send()
-
-        def one(g, unused):
-            pass_f(g).wait_send()
-            return unused
-
-        lax.fori_loop(0, groups, one, 0)
-
-    @pl.when(has_last)
-    def _():
-        edge(1).wait_send()
-
-        def one(g, unused):
-            pass_b(g).wait_send()
-            return unused
-
-        lax.fori_loop(0, groups, one, 0)
-
-
-def mixer(n, signal, write, read, gate, gain, steps, conv_x, conv_b, conv_c, rates):
+        for k in range(3):
+            give_tap(k, i).wait_send()
+        give_rate(i).wait_send()
+
+    @pl.when(sends_up)
+    def _():
+        for k in range(3):
+            for to in range(inner):
+                give_halo(0, k, to).wait_send()
+
+    @pl.when(sends_down)
+    def _():
+        for k in range(3):
+            for to in range(inner):
+                give_halo(1, k, to).wait_send()
+
+    def drain(q, unused):
+        for k in range(3):
+            for i in range(1, inner):
+                give_in(k, q, i).wait_send()
+        for i in range(1, inner):
+            give_y(q, lax.rem(x + i, inner)).wait_send()
+
+        @pl.when(has_above)
+        def _():
+            pass_f(q).wait_send()
+
+        @pl.when(has_below)
+        def _():
+            pass_b(q).wait_send()
+
+        return unused
+
+    lax.fori_loop(0, locals_n, drain, 0)
+    for offset in range(dp_count):
+        for bit in bits:
+            if offset == 0 or bit < lowest(offset):
+                for c in range(pieces):
+                    give_weight(offset, bit, c).wait_send()
+
+
+def mixer(
+    n, inner, dp_count, signal, write, read, gate, residual, weight, steps,
+    conv_x, conv_b, conv_c, rates, gain, ffn_gain,
+):
     f32, bf16 = jnp.float32, jnp.bfloat16
     tokens, width = signal.shape
     groups = write.shape[1] // STATE
     lanes = width // groups
-    taps_n, wide = conv_x.shape
-    half = taps_n // 2
-    columns = steps.shape[1]
-    padded = max(columns, BLOCK)
-    own = rates.T.reshape(1, -1)
-    row = jnp.zeros((1, wide), f32)
-    row = lax.dynamic_update_slice(row, own, (0, lax.axis_index("sp") * own.shape[1]))
-    lines = 3 * taps_n + 1
-    spare = -lines % 8
-    taps = jnp.concatenate([conv_x, conv_b, conv_c, row, jnp.zeros((spare, wide), f32)], axis=0)
-    few = [signal, write, read]
-    blank = jnp.zeros((16 - 3 * half, width), bf16)
-    edges = jnp.stack(
-        [
-            jnp.concatenate([v[tokens - half :] for v in few] + [blank], axis=0),
-            jnp.concatenate([v[:half] for v in few] + [blank], axis=0),
-        ]
-    )
-    step = jnp.pad(steps.astype(f32), ((0, 0), (0, padded - columns)))
+    own = groups // inner
+    span = width // inner
+    depth = weight.shape[0]
+    pieces = depth // min(depth, 128)
+    bits = dp_count.bit_length() - 1
     inside = pl.BlockSpec(memory_space=pltpu.VMEM)
+    anywhere = pl.BlockSpec(memory_space=pl.ANY)
     dma = pltpu.SemaphoreType.DMA
-    tile = pltpu.VMEM((groups, tokens, lanes), f32)
-    state = pltpu.VMEM((groups, STATE, lanes), f32)
-    small = pltpu.VMEM((groups, STATE, lanes), bf16)
+    vmem = pltpu.VMEM
+    tile = vmem((own, inner, tokens, lanes), f32)
+    state = vmem((own, inner, STATE, lanes), f32)
+    small = vmem((own, STATE, lanes), bf16)
+    flat = vmem((tokens, width), bf16)
     return pl.pallas_call(
-        functools.partial(mixer_kernel, n, taps_n),
-        out_shape=jax.ShapeDtypeStruct((tokens, width), bf16),
-        in_specs=[inside] * 8,
-        out_specs=inside,
+        functools.partial(mixer_kernel, n, inner, dp_count),
+        out_shape=(
+            jax.ShapeDtypeStruct((tokens, width), f32),
+            jax.ShapeDtypeStruct((tokens, width), bf16),
+        ),
+        in_specs=[anywhere] * 6 + [inside] * 7,
+        out_specs=(inside, inside),
         scratch_shapes=[
-            pltpu.VMEM((lines + spare, n * wide), f32),
-            pltpu.VMEM(edges.shape, bf16),
-            pltpu.VMEM(edges.shape, f32),
-            pltpu.VMEM((3, tokens + 16, lanes), f32),
-            pltpu.VMEM((groups, tokens, STATE), bf16),
+            vmem((3, inner, tokens, span), bf16), flat, flat,
+            vmem((dp_count, depth, width), bf16),
+            vmem((inner,) + steps.shape, bf16),
+            vmem((3, 8, width), f32),
+            vmem((n,) + rates.shape, f32),
+            vmem((2, 3, 8, span), bf16),
+            vmem((2, 3, 8, span), f32),
+            vmem((3, inner * tokens + 16, lanes), f32),
+            vmem((own, inner, tokens, STATE), bf16),
             tile, tile, tile, state, state,
-            pltpu.VMEM((groups, 8, lanes), f32),
-            small, small, small, small, tile,
-            pltpu.VMEM((3, groups, tokens, 8), f32),
-            pltpu.VMEM((3, groups, 8, tokens), f32),
-            pltpu.VMEM((NORM_GROUPS, tokens, 1), f32),
-            dma((n,)), dma((n,)), dma((2,)), dma((2,)),
-            dma((groups,)), dma((groups,)), dma((groups,)), dma((groups,)), dma((1,)),
+            vmem((own, inner, 8, lanes), f32),
+            small, small, small, small,
+            vmem((own, inner, tokens, lanes), bf16), flat,
+            vmem((groups, tokens, lanes), f32), flat,
+            vmem((3, inner, own, tokens, 8), f32),
+            vmem((3, inner, own, 8, tokens), f32),
+            vmem((NORM_GROUPS, tokens, 1), f32),
+            dma((3, own, inner)), dma((3, own, inner)), dma((inner,)), dma((inner,)),
+            dma((3, n)), dma((3, n)), dma((n,)), dma((n,)), dma((2, 3, inner)), dma((2, 3)),
+            dma((own,)), dma((own,)), dma((own,)), dma((own,)),
+            dma((inner, own)), dma((inner, own)),
+            dma((dp_count, bits, pieces)), dma((dp_count, pieces)), dma((3,)), dma((8,)),
         ],
         compiler_params=pltpu.CompilerParams(
-            collective_id=1, has_side_effects=True, vmem_limit_bytes=40 * 1024 * 1024
+            collective_id=1, has_side_effects=True, vmem_limit_bytes=56 * 1024 * 1024
         ),
         cost_estimate=pl.CostEstimate(
             flops=40 * 10**9, bytes_accessed=4 * tokens * width * 2, transcendentals=0
         ),
         name="mixer",
-    )(signal, write, read, gate, gain.reshape(1, width), step, edges, taps)
-
-
-def scale_rows(values, gains):
-    return values * lax.rsqrt(jnp.mean(values * values, axis=-1, keepdims=True) + epsilon) * gains
-
-
-def gather_rows(weight, count):
-    parts = {0: weight}
-    step = count // 2
-    while step >= 1:
-        pairs = [(d, d ^ step) for d in range(count)]
-        for offset, block in list(parts.items()):
-            parts[offset ^ step] = lax.ppermute(block, "dp", pairs)
-        step //= 2
-    return parts
+    )(
+        signal, write, read, gate, residual, weight, steps, conv_x, conv_b, conv_c, rates,
+        gain.reshape(1, width), ffn_gain.reshape(1, width),
+    )
 
 
 def per_device(
@@ -694,23 +919,14 @@
     sp_count = lax.axis_size("sp")
     dp_count = lax.axis_size("dp")
     bf16, f32 = jnp.bfloat16, jnp.float32
-    parts = gather_rows(out_weight, dp_count)
-    mixed = mixer(
-        sp_count, ssm_input[0], state_b[0], state_c[0], gate_input[0], mix_gain, step_raw[0],
-        conv_x, conv_b, conv_c, decay_rate,
+    inner = dp_count // 2
+    token_count = residual_in.shape[1]
+    stream, ffn_input = mixer(
+        sp_count, inner, dp_count, ssm_input[0], state_b[0], state_c[0], gate_input[0],
+        residual_in[0], out_weight, step_raw[0], conv_x, conv_b, conv_c, decay_rate,
+        mix_gain, ffn_gain,
     )
-
-    token_count = residual_in.shape[1]
-    depth = out_weight.shape[0]
-    me = lax.axis_index("dp")
-    stream = residual_in[0].astype(f32)
-    for offset, block in parts.items():
-        piece = lax.dynamic_slice_in_dim(mixed, (me ^ offset) * depth, depth, axis=1)
-        stream = stream + jnp.dot(piece, block, preferred_element_type=f32)
-    ffn_input = scale_rows(stream, ffn_gain).astype(bf16)
-
     top_count = routing.shape[2]
-    inner = dp_count // 2
     planes = sp_count // inner
     capacity = 4 * token_count * top_count // (2 * sp_count * dp_count)
     info = jnp.concatenate([routing[0].T.astype(f32), route_weight[0].T], axis=0)

time: 259 us -> 188 us (0.73)
  waiting for transfers between devices: 39.6 us -> 0 us
  Pallas kernels: 194 us -> 182 us
  local copies, waits for them, and re-layouts: 10.8 us -> 1.44 us
  matrix products: 6.67 us -> 0 us
  starting transfers between devices: 2.71 us -> 0 us
    ppermute x3 -> x0, waiting for transfers between devices: 39.6 us -> none  [gather_rows(): parts[offset ^ step] = lax.ppermute(block, 'dp', pairs)]
    pallas_call x1, Pallas kernels: 138 us -> 126 us  [experts(): pl.pallas_call(functools.partial(experts_kernel, planes, inner, dp_count,...]
    dot_general x4 -> x0, matrix products: 6.67 us -> none  [per_device(): stream = stream + jnp.dot(piece, block, preferred_element_type=f32)]
    unnamed x21 -> x3, local copies, waits for them, and re-layouts: 5.71 us -> 1.44 us
    ppermute x3 -> x0, starting transfers between devices: 2.71 us -> none  [gather_rows(): parts[offset ^ step] = lax.ppermute(block, 'dp', pairs)]
  transfers between devices with their start and end apart: 3 -> 0, of which waited for: 1 -> 0; matrix products, arithmetic and copies ran while one was open for 4% -> 0% of each run, Pallas kernels for 22% -> 0%
where the time goes in v3:
time: 188 us
  Pallas kernels  182 us (97%)
  other arithmetic  4.1 us (2%)
    pallas_call x1, Pallas kernels, experts(): pl.pallas_call(functools.partial(experts_kernel, planes, inner, dp_count,...  126 us
    pallas_call x1, Pallas kernels, mixer(): pl.pallas_call(functools.partial(mixer_kernel, n, inner, dp_count), out_s...  56.2 us

profile of v3, /device:TPU:29, one launch (start us, length us, event | category | flops | bytes accessed | tf_op | source)
XLA Modules:
  0.0 187.9 jit_solution(303778110729668872)
XLA Ops:
  0.0 0.7 convert_bitcast_fusion
  0.7 1.3 pad_maximum_fusion.info_ref
  2.0 1.4 copy.19
  3.4 56.2 %mixer.1 = (f32[128,2048]{1,0:T(8,128)}, bf16[128,2048]{1,0:T(8,128)(2,1)}) custom-call(bf16[128,2048]{1,0:T(8,128)(2,1)} %bitcast.19, bf16[128,2048]{1,0:T(8,128)(2,1)} %bitcast.20, bf16[128,2048]{1,0:T(8,128)(2,1)} %bitcast.21, bf16[128,2048]{1,0:T(8,128)(2,1)} %bitcast.22, bf16[128,2048]{1,0:T(8,128)(2,1)} %bitcast.23, bf16[512,2048]{1,0:T(8,128)(2,1)} %w_hbm.1, ...), custom_call_target="tpu_custom_call" | custom-call | flops 40000000000 | bytes 2097152 | tf_op jit(solution)/shard_map/mixer/pallas_call | solution.py:870
  59.6 0.0 copy-start
  59.6 126.1 %experts.1 = f32[128,2048]{1,0:T(8,128)} custom-call(bf16[128,2048]{1,0:T(8,128)(2,1)} %get-tuple-element.8.x_ref, f32[8,128]{1,0:T(8,128)} %pad_maximum_fusion.info_ref, bf16[1,2048,1024]{2,1,0:T(8,128)(2,1)} %gate_hbm.1, bf16[1,2048,1024]{2,1,0:T(8,128)(2,1)} %up_hbm.1, bf16[1,1024,2048]{2,1,0:T(8,128)(2,1)} %down_hbm.1), custom_call_target="tpu_custom_call" | custom-call | flops 99999997952 | bytes 100000000 | tf_op jit(solution)/shard_map/experts/pallas_call | solution.py:321
  185.7 0.0 copy-done
  185.8 2.1 %fusion = bf16[1,128,2048]{2,1,0:T(8,128)(2,1)} fusion(f32[128,2048]{1,0:T(8,128)S(1)} %copy-done, f32[128,2048]{1,0:T(8,128)} %experts.1), kind=kLoop, calls=%fused_computation.1 | loop fusion | flops 524288 | bytes 2621440 | tf_op jit(solution)/shard_map/broadcast_in_dim | solution.py:936
Async XLA Ops:
  59.6 126.2 %copy-start = (f32[128,2048]{1,0:T(8,128)S(1)}, f32[128,2048]{1,0:T(8,128)}, u32[]{:S(2)}) copy-start(f32[128,2048]{1,0:T(8,128)} %get-tuple-element.7) | copy-start | bytes 3145732

commit v4 on v3

--- a/solution.py
+++ b/solution.py
@@ -30,15 +30,18 @@
     below, above = z, planes - 1 - z
     both = jnp.minimum(below, above)
     near = (s + 1) // 2
-    from_below = jnp.where(s <= 2 * both, s % 2, jnp.where(below > above, 1, 0))
+    low = jnp.where(below < above, 1, 0)
+    turn = jnp.where(low == 1, s % 2, 1 - s % 2)
+    from_below = jnp.where(s <= 2 * both, turn, 1 - low)
     hops = jnp.where(s <= 2 * both, near, s - both)
     return hops, from_below, z + hops * (1 - 2 * from_below)
 
 
 def experts_kernel(
-    planes, inner, dp_count, top, x_ref, info_ref, gate_hbm, up_hbm, down_hbm, out_ref,
-    gate, up, down, tok, infos, rows_out, rows_in, made, back, high, low, active, part, part_in,
-    wsem, isend, irecv, zsend, zrecv, dsend, drecv, rsend, rrecv, psend, precv, local,
+    planes, inner, dp_count, top, x_ref, stream_ref, names_ref, shares_ref, gate_hbm, up_hbm,
+    down_hbm, out_ref, gate, up, down, tok, names_in, shares_in, rows_out, rows_in, made, back, high, low, active, part, part_in,
+    total, passing, wsem, isend, irecv, zsend, zrecv, dsend, drecv, rsend, rrecv, psend, precv,
+    csend, crecv, local,
 ):
     f32, bf16 = jnp.float32, jnp.bfloat16
     near = inner * dp_count
@@ -75,18 +78,19 @@
         load.start()
     pl.semaphore_wait(barrier, near - 1 + planes - 1)
 
-    def tell(i):
+    def tell(kind, i):
         return pltpu.make_async_remote_copy(
-            src_ref=info_ref,
-            dst_ref=infos.at[z],
-            send_sem=isend.at[i],
-            recv_sem=irecv.at[i],
+            src_ref=(names_ref, shares_ref)[kind],
+            dst_ref=(names_in, shares_in)[kind].at[z],
+            send_sem=isend.at[kind, i],
+            recv_sem=irecv.at[kind, i],
             device_id=plane(lax.rem(z + i, planes)),
             device_id_type=MESH,
         )
 
     for i in range(1, planes):
-        tell(i).start()
+        for kind in range(2):
+            tell(kind, i).start()
 
     def along(src, block, step, way):
         return pltpu.make_async_remote_copy(
@@ -111,7 +115,7 @@
     ti = lax.broadcasted_iota(jnp.int32, (tokens, tokens), 0)
     tj = lax.broadcasted_iota(jnp.int32, (tokens, tokens), 1)
     earlier = jnp.where(ti < tj, 1.0, 0.0).astype(bf16)
-    expert = (z * near + lax.broadcasted_iota(jnp.int32, (near, tokens), 0)).astype(f32)
+    expert = z * near + lax.broadcasted_iota(jnp.int32, (near, tokens), 0)
     place_in = lax.broadcasted_iota(jnp.int32, (near, cap, tokens), 1).astype(f32)
 
     def send_rows(block, i):
@@ -151,8 +155,7 @@
 
         lax.fori_loop(1, near, one, 0)
 
-    def dispatch(block, values, info):
-        names, weights = info[0:top, :], info[top : 2 * top, :]
+    def dispatch(block, values, names, weights):
         named, weight = None, None
         for k in range(top):
             hit = names[k : k + 1, :] == expert
@@ -190,8 +193,9 @@
             along(tok.at[block], block, hops, way).start()
 
         source = lax.rem(z - block + planes, planes)
-        tell(source).wait_recv()
-        dispatch(block, tok[block], infos[block])
+        for kind in range(2):
+            tell(kind, source).wait_recv()
+        dispatch(block, tok[block], names_in[block], shares_in[block])
         return block
 
     hidden = gate.shape[1]
@@ -232,13 +236,36 @@
             high[block], rows, dims, preferred_element_type=f32
         ) + lax.dot_general(low[block], rows, dims, preferred_element_type=f32)
 
-    def send_part(block, i):
+    chunk = 512
+    chunks = width // chunk
+
+    def send_part(block, i, c):
         return pltpu.make_async_remote_copy(
-            src_ref=part.at[block],
-            dst_ref=part_in.at[z],
-            send_sem=psend.at[i],
-            recv_sem=precv.at[i],
+            src_ref=part.at[block, :, c * chunk : (c + 1) * chunk],
+            dst_ref=part_in.at[z, :, c * chunk : (c + 1) * chunk],
+            send_sem=psend.at[i, c],
+            recv_sem=precv.at[i, c],
             device_id=plane(block),
+            device_id_type=MESH,
+        )
+
+    middle = planes // 2
+    in_low = z < middle
+    outermost = (z == 0) | (z == planes - 1)
+    innermost = (z == middle - 1) | (z == middle)
+    inward = jnp.where(in_low, z + 1, z - 1)
+
+    def is_far(block):
+        return in_low == (block >= middle)
+
+    def pass_on(block, c):
+        slot = lax.rem(block, middle)
+        return pltpu.make_async_remote_copy(
+            src_ref=part.at[block, :, c * chunk : (c + 1) * chunk],
+            dst_ref=passing.at[slot, :, c * chunk : (c + 1) * chunk],
+            send_sem=csend.at[slot, c],
+            recv_sem=crecv.at[slot, c],
+            device_id=plane(inward),
             device_id_type=MESH,
         )
 
@@ -248,13 +275,32 @@
 
     def collect(block):
         landed(block)
-        chunk = 512
-        for at in range(0, width, chunk):
-            part[block, :, at : at + chunk] = gathered(block, at, chunk).astype(bf16)
-        send_part(block, lax.rem(block - z + planes, planes)).start()
+        adds = is_far(block) & jnp.logical_not(outermost)
+        inner_far = is_far(block) & jnp.logical_not(innermost)
+        slot = lax.rem(block, middle)
+        for c in range(chunks):
+            at = c * chunk
+
+            @pl.when(adds)
+            def _():
+                pass_on(block, c).wait_recv()
+                value = gathered(block, at, chunk) + passing[slot, :, at : at + chunk].astype(f32)
+                part[block, :, at : at + chunk] = value.astype(bf16)
+
+            @pl.when(jnp.logical_not(adds))
+            def _():
+                part[block, :, at : at + chunk] = gathered(block, at, chunk).astype(bf16)
+
+            @pl.when(inner_far)
+            def _():
+                pass_on(block, c).start()
+
+            @pl.when(jnp.logical_not(inner_far))
+            def _():
+                send_part(block, lax.rem(block - z + planes, planes), c).start()
 
     blocks = [z]
-    dispatch(z, x_ref[...], info_ref[...])
+    dispatch(z, x_ref[...], names_ref[...], shares_ref[...])
     served = 0
     for s in range(1, planes):
         blocks.append(arrive(s))
@@ -267,23 +313,58 @@
         for load in loads:
             load.wait()
         serve(blocks[0])
-    for s in range(1, planes):
+    last = list(range(middle, planes))
+    first = list(range(1, middle))
+    for s in last[:-1]:
         serve(blocks[s])
         give(blocks[s])
+    for s in first:
+        serve(blocks[s])
+    for s in last[-1:]:
+        serve(blocks[s])
+        give(blocks[s])
+    for s in first:
+        give(blocks[s])
     give(blocks[0])
-    for s in range(1, planes):
+    for s in last + first:
         collect(blocks[s])
     landed(z)
-    chunk = 512
     for at in range(0, width, chunk):
-        out_ref[:, at : at + chunk] = gathered(z, at, chunk)
+        cols = slice(at, at + chunk)
+        total[:, cols] = stream_ref[:, cols] + gathered(z, at, chunk)
+
+    def comes(source):
+        near_by = jnp.logical_not(is_far(source))
+        edge = (source == middle - 1) | (source == middle)
+        return near_by | edge
+
     for i in range(1, planes):
-        send_part(lax.rem(z + i, planes), i).wait_recv()
-        out_ref[...] += part_in[lax.rem(z - i + planes, planes)].astype(f32)
-
+        source = lax.rem(z - i + planes, planes)
+
+        @pl.when(comes(source))
+        def _():
+            for c in range(chunks):
+                cols = slice(c * chunk, (c + 1) * chunk)
+                send_part(lax.rem(z + i, planes), i, c).wait_recv()
+                total[:, cols] += part_in[source, :, cols].astype(f32)
+
+    out_ref[...] = total[...].astype(bf16)
     for i in range(1, planes):
-        tell(i).wait_send()
-        send_part(lax.rem(z + i, planes), i).wait_send()
+        for kind in range(2):
+            tell(kind, i).wait_send()
+        block = lax.rem(z + i, planes)
+        inner_far = is_far(block) & jnp.logical_not(innermost)
+
+        @pl.when(inner_far)
+        def _():
+            for c in range(chunks):
+                pass_on(block, c).wait_send()
+
+        @pl.when(jnp.logical_not(inner_far))
+        def _():
+            for c in range(chunks):
+                send_part(block, i, c).wait_send()
+
     for block in range(planes):
         each(lambda i: send_rows(block, i).wait_send())
         each(lambda i: send_back(block, i).wait_send())
@@ -307,7 +388,9 @@
             along(tok.at[z], z, step, 1).wait_send()
 
 
-def experts(planes, inner, dp_count, cap, top, tokens_in, info, gate_w, up_w, down_w):
+def experts(
+    planes, inner, dp_count, cap, tokens_in, stream, names, shares, gate_w, up_w, down_w
+):
     near = inner * dp_count
     tokens, width = tokens_in.shape
     hidden = gate_w.shape[2]
@@ -319,29 +402,33 @@
     table = pltpu.VMEM((planes, near * cap, tokens), bf16)
     blocks = pltpu.VMEM((planes, tokens, width), bf16)
     return pl.pallas_call(
-        functools.partial(experts_kernel, planes, inner, dp_count, top),
-        out_shape=jax.ShapeDtypeStruct((tokens, width), f32),
-        in_specs=[inside, inside, anywhere, anywhere, anywhere],
+        functools.partial(experts_kernel, planes, inner, dp_count, names.shape[0]),
+        out_shape=jax.ShapeDtypeStruct((tokens, width), bf16),
+        in_specs=[inside] * 4 + [anywhere] * 3,
         out_specs=inside,
         scratch_shapes=[
             pltpu.VMEM((width, hidden), bf16),
             pltpu.VMEM((width, hidden), bf16),
             pltpu.VMEM((hidden, width), bf16),
             blocks,
-            pltpu.VMEM((planes,) + info.shape, f32),
+            pltpu.VMEM((planes,) + names.shape, names.dtype),
+            pltpu.VMEM((planes,) + shares.shape, f32),
             rows, rows, rows, rows, table, table,
             pltpu.VMEM((near * cap, hidden), bf16),
             blocks, blocks,
-            dma((3,)), dma((planes,)), dma((planes,)), dma((2, planes)), dma((2, planes)),
+            pltpu.VMEM((tokens, width), f32),
+            pltpu.VMEM((planes // 2, tokens, width), bf16),
+            dma((3,)), dma((2, planes)), dma((2, planes)), dma((2, planes)), dma((2, planes)),
             dma((planes, near)), dma((planes, near)), dma((planes, near)), dma((planes, near)),
-            dma((planes,)), dma((planes,)), dma((2, planes)),
+            dma((planes, width // 512)), dma((planes, width // 512)),
+            dma((planes // 2, width // 512)), dma((planes // 2, width // 512)), dma((2, planes)),
         ],
         compiler_params=pltpu.CompilerParams(
             collective_id=3, has_side_effects=True, vmem_limit_bytes=60 * 1024 * 1024
         ),
         cost_estimate=pl.CostEstimate(flops=10**11, bytes_accessed=10**8, transcendentals=0),
         name="experts",
-    )(tokens_in, info, gate_w, up_w, down_w)
+    )(tokens_in, stream, names, shares, gate_w, up_w, down_w)
 
 
 def lowest(offset):
@@ -517,7 +604,7 @@
         copy.wait()
     for i in range(1, n):
         give_rate(i).wait_recv()
-    step_columns = step_ref.shape[1]
+    step_columns = step_ref.shape[0]
     window = step_columns // inner
     held = rate_ref.shape[1]
     rate = jnp.zeros((1, BLOCK), f32)
@@ -536,7 +623,9 @@
     for i in range(1, inner):
         give_step(i).wait_recv()
     for i in range(inner):
-        v = jnp.dot(steps[i], choose, preferred_element_type=f32)
+        v = lax.dot_general(
+            steps[i], choose, (((0,), (0,)), ((), ())), preferred_element_type=f32
+        )
         dt = jnp.maximum(v, 0.0) + jnp.log(1.0 + jnp.exp(-jnp.abs(v)))
         a = dt * rate
         inc = jnp.dot(lower, a, precision=highest, preferred_element_type=f32)
@@ -698,8 +787,9 @@
             def _():
                 give_y(q, i).start()
 
-    late_f = (3 * z + 1) // 2
-    late_b = (3 * (planes - 1 - z) + 1) // 2
+    gap = 2
+    late_f = gap * z
+    late_b = gap * (planes - 1 - z)
     late = jnp.maximum(late_f, late_b)
 
     def turn(t, unused):
@@ -734,7 +824,7 @@
 
         return unused
 
-    lax.fori_loop(0, locals_n + (3 * (planes - 1) + 1) // 2, turn, 0)
+    lax.fori_loop(0, locals_n + gap * (planes - 1), turn, 0)
 
     per_norm = groups // NORM_GROUPS
     squares[...] = jnp.zeros(squares.shape, f32)
@@ -772,27 +862,40 @@
 
     stream_ref[...] = res_v[...].astype(f32)
     order = sorted(range(1, dp_count), key=lambda o: (-lowest(o), o))
-    for offset in [0] + order:
-        if offset:
-            for c in range(pieces):
-                give_weight(offset - lowest(offset), lowest(offset), c).wait_recv()
-                for bit in bits:
-                    if bit < lowest(offset):
-                        give_weight(offset, bit, c).start()
+
+    def come(offset, c):
+        give_weight(offset - lowest(offset), lowest(offset), c).wait_recv()
+        for bit in bits:
+            if bit < lowest(offset):
+                give_weight(offset, bit, c).start()
+
+    def project(offset, first, last):
         block = dp
         for bit in bits:
             if offset & bit:
                 block = block + bit * (1 - 2 * lax.rem(dp // bit, 2))
-        part = mixed[:, spot(block * depth, depth)]
-
-        def project(t, unused):
+        part = mixed[:, pl.ds(pl.multiple_of(block * depth + first, 128), last - first)]
+
+        def tile(t, unused):
             at = spot(t * 512, 512)
             stream_ref[:, at] += jnp.dot(
-                part, w_all[offset, :, at], preferred_element_type=f32
+                part, w_all[offset, first:last, at], preferred_element_type=f32
             )
             return unused
 
-        lax.fori_loop(0, width // 512, project, 0)
+        lax.fori_loop(0, width // 512, tile, 0)
+
+    early = depth - piece
+    for offset in order:
+        for c in range(pieces - 1):
+            come(offset, c)
+    project(0, 0, depth)
+    for offset in order:
+        if early:
+            project(offset, 0, early)
+    for offset in order:
+        come(offset, pieces - 1)
+        project(offset, early, depth)
     total = jnp.zeros((tokens, 1), f32)
     for at in range(0, width, 512):
         value = stream_ref[:, at : at + 512]
@@ -918,22 +1021,20 @@
 ):
     sp_count = lax.axis_size("sp")
     dp_count = lax.axis_size("dp")
-    bf16, f32 = jnp.bfloat16, jnp.float32
     inner = dp_count // 2
     token_count = residual_in.shape[1]
     stream, ffn_input = mixer(
         sp_count, inner, dp_count, ssm_input[0], state_b[0], state_c[0], gate_input[0],
-        residual_in[0], out_weight, step_raw[0], conv_x, conv_b, conv_c, decay_rate,
+        residual_in[0], out_weight, step_raw[0].T, conv_x, conv_b, conv_c, decay_rate,
         mix_gain, ffn_gain,
     )
     top_count = routing.shape[2]
     planes = sp_count // inner
     capacity = 4 * token_count * top_count // (2 * sp_count * dp_count)
-    info = jnp.concatenate([routing[0].T.astype(f32), route_weight[0].T], axis=0)
-    routed = experts(
-        planes, inner, dp_count, capacity, top_count, ffn_input, info, gate_w, up_w, down_w
-    )
-    return (stream + routed).astype(bf16)[None]
+    return experts(
+        planes, inner, dp_count, capacity, ffn_input, stream, routing[0].T, route_weight[0].T,
+        gate_w, up_w, down_w,
+    )[None]
 
 
 def solution(mesh):

time: 188 us -> 171 us (0.910); the launches traced: 188 us -> 168 us
  Pallas kernels: 182 us -> 167 us
  other arithmetic: 4.1 us -> 0 us
    pallas_call x1, Pallas kernels: 126 us -> 111 us  [experts(): pl.pallas_call(functools.partial(experts_kernel, planes, inner, dp_count,...]
    broadcast_in_dim x1 -> x0, other arithmetic: 2.14 us -> none  [per_device(): return (stream + routed).astype(bf16)[None]]
where the time goes in v4:
time: 171 us; the launch traced here: 168 us
  Pallas kernels  167 us (98%)
  local copies, waits for them, and re-layouts  1.88 us (1%)
    pallas_call x1, Pallas kernels, experts(): pl.pallas_call(functools.partial(experts_kernel, planes, inner, dp_count,...  111 us
    pallas_call x1, Pallas kernels, mixer(): pl.pallas_call(functools.partial(mixer_kernel, n, inner, dp_count), out_s...  55.9 us

profile of v4, /device:TPU:29, one launch (start us, length us, event | category | flops | bytes accessed | tf_op | source)
XLA Modules:
  0.0 168.5 jit_solution(9490301012488589691)
XLA Ops:
  0.0 55.9 %mixer.1 = (f32[128,2048]{1,0:T(8,128)}, bf16[128,2048]{1,0:T(8,128)(2,1)}) custom-call(bf16[128,2048]{1,0:T(8,128)(2,1)} %bitcast.18, bf16[128,2048]{1,0:T(8,128)(2,1)} %bitcast.19, bf16[128,2048]{1,0:T(8,128)(2,1)} %bitcast.20, bf16[128,2048]{1,0:T(8,128)(2,1)} %bitcast.21, bf16[128,2048]{1,0:T(8,128)(2,1)} %bitcast.22, bf16[512,2048]{1,0:T(8,128)(2,1)} %w_hbm.1, ...), custom_call_target="tpu_custom_call" | custom-call | flops 40000000000 | bytes 2097152 | tf_op jit(solution)/shard_map/mixer/pallas_call | solution.py:973
  55.9 110.7 %experts.1 = bf16[128,2048]{1,0:T(8,128)(2,1)} custom-call(bf16[128,2048]{1,0:T(8,128)(2,1)} %get-tuple-element.7.x_ref, f32[128,2048]{1,0:T(8,128)} %get-tuple-element.8.stream_ref, s32[4,128]{1,0:T(4,128)} %bitcast.26, f32[4,128]{1,0:T(4,128)} %bitcast.27, bf16[1,2048,1024]{2,1,0:T(8,128)(2,1)} %gate_hbm.1, bf16[1,2048,1024]{2,1,0:T(8,128)(2,1)} %up_hbm.1, ...), custom_call_target="tpu_custom_call" | custom-call | flops 99999997952 | bytes 100000000 | tf_op jit(solution)/shard_map/experts/pallas_call | solution.py:404
  166.6 1.9 %copy.20 = bf16[1,128,2048]{2,1,0:T(8,128)(2,1)} copy(bf16[1,128,2048]{2,1,0:T(8,128)(2,1)} %bitcast.17) | data formatting | bytes 1048576

commit v5 on v4

--- a/solution.py
+++ b/solution.py
@@ -92,12 +92,16 @@
         for kind in range(2):
             tell(kind, i).start()
 
-    def along(src, block, step, way):
+    parts_n = 2
+    share = width // parts_n
+
+    def along(src, block, step, way, c):
+        cut = slice(c * share, (c + 1) * share)
         return pltpu.make_async_remote_copy(
-            src_ref=src,
-            dst_ref=tok.at[block],
-            send_sem=zsend.at[way, step],
-            recv_sem=zrecv.at[way, step],
+            src_ref=src.at[:, cut],
+            dst_ref=tok.at[block, :, cut],
+            send_sem=zsend.at[way, step, c],
+            recv_sem=zrecv.at[way, step, c],
             device_id=plane(z + 1 - 2 * way),
             device_id_type=MESH,
         )
@@ -106,11 +110,13 @@
 
     @pl.when(up_open)
     def _():
-        along(x_ref, z, 0, 0).start()
+        for c in range(parts_n):
+            along(x_ref, z, 0, 0, c).start()
 
     @pl.when(down_open)
     def _():
-        along(x_ref, z, 0, 1).start()
+        for c in range(parts_n):
+            along(x_ref, z, 0, 1, c).start()
 
     ti = lax.broadcasted_iota(jnp.int32, (tokens, tokens), 0)
     tj = lax.broadcasted_iota(jnp.int32, (tokens, tokens), 1)
@@ -118,13 +124,14 @@
     expert = z * near + lax.broadcasted_iota(jnp.int32, (near, tokens), 0)
     place_in = lax.broadcasted_iota(jnp.int32, (near, cap, tokens), 1).astype(f32)
 
-    def send_rows(block, i):
+    def send_rows(block, i, c):
         peer = lax.rem(me + i, near)
+        cut = slice(c * share, (c + 1) * share)
         return pltpu.make_async_remote_copy(
-            src_ref=rows_out.at[block, peer],
-            dst_ref=rows_in.at[block, me],
-            send_sem=dsend.at[block, i],
-            recv_sem=drecv.at[block, i],
+            src_ref=rows_out.at[block, peer, :, cut],
+            dst_ref=rows_in.at[block, me, :, cut],
+            send_sem=dsend.at[block, i, c],
+            recv_sem=drecv.at[block, i, c],
             device_id=place(peer),
             device_id_type=MESH,
         )
@@ -155,7 +162,7 @@
 
         lax.fori_loop(1, near, one, 0)
 
-    def dispatch(block, values, names, weights):
+    def choose(block, names, weights):
         named, weight = None, None
         for k in range(top):
             hit = names[k : k + 1, :] == expert
@@ -174,28 +181,32 @@
 
         high[block] = table(rough[:, None, :])
         low[block] = table(rest[:, None, :])
-        select = table(jnp.ones((near, 1, tokens), f32))
-        chunk = 512
-        for at in range(0, width, chunk):
-            rows = jnp.dot(select, values[:, at : at + chunk], preferred_element_type=f32)
-            rows_out[block, :, :, at : at + chunk] = rows.astype(bf16).reshape(near, cap, chunk)
-        each(lambda i: send_rows(block, i).start())
-        keep_rows(block).start()
+        return table(jnp.ones((near, 1, tokens), f32))
+
+    def dispatch(block, select, ref, c):
+        for at in range(c * share, (c + 1) * share, 512):
+            rows = jnp.dot(select, ref[:, at : at + 512], preferred_element_type=f32)
+            rows_out[block, :, :, at : at + 512] = rows.astype(bf16).reshape(near, cap, 512)
+        each(lambda i: send_rows(block, i, c).start())
+        if c == parts_n - 1:
+            keep_rows(block).start()
 
     def arrive(s):
         hops, from_below, block = plane_order(z, planes, s)
         way = 1 - from_below
-        along(tok.at[block], block, hops - 1, way).wait_recv()
         onward = jnp.where(from_below == 1, z + 1, z - 1)
-
-        @pl.when((onward >= 0) & (onward < planes))
-        def _():
-            along(tok.at[block], block, hops, way).start()
-
         source = lax.rem(z - block + planes, planes)
         for kind in range(2):
             tell(kind, source).wait_recv()
-        dispatch(block, tok[block], names_in[block], shares_in[block])
+        select = choose(block, names_in[block], shares_in[block])
+        for c in range(parts_n):
+            along(tok.at[block], block, hops - 1, way, c).wait_recv()
+
+            @pl.when((onward >= 0) & (onward < planes))
+            def _():
+                along(tok.at[block], block, hops, way, c).start()
+
+            dispatch(block, select, tok.at[block], c)
         return block
 
     hidden = gate.shape[1]
@@ -203,7 +214,8 @@
 
     def serve(block):
         keep_rows(block).wait()
-        each(lambda i: send_rows(block, i).wait_recv())
+        for c in range(parts_n):
+            each(lambda i: send_rows(block, i, c).wait_recv())
         tile = 256
 
         def lift(n, carry):
@@ -300,7 +312,9 @@
                 send_part(block, lax.rem(block - z + planes, planes), c).start()
 
     blocks = [z]
-    dispatch(z, x_ref[...], names_ref[...], shares_ref[...])
+    select = choose(z, names_ref[...], shares_ref[...])
+    for c in range(parts_n):
+        dispatch(z, select, x_ref, c)
     served = 0
     for s in range(1, planes):
         blocks.append(arrive(s))
@@ -366,26 +380,31 @@
                 send_part(block, i, c).wait_send()
 
     for block in range(planes):
-        each(lambda i: send_rows(block, i).wait_send())
+        for c in range(parts_n):
+            each(lambda i: send_rows(block, i, c).wait_send())
         each(lambda i: send_back(block, i).wait_send())
 
     @pl.when(up_open)
     def _():
-        along(x_ref, z, 0, 0).wait_send()
+        for c in range(parts_n):
+            along(x_ref, z, 0, 0, c).wait_send()
 
     @pl.when(down_open)
     def _():
-        along(x_ref, z, 0, 1).wait_send()
+        for c in range(parts_n):
+            along(x_ref, z, 0, 1, c).wait_send()
 
     for step in range(1, planes):
 
         @pl.when(up_open & (z - step >= 0))
         def _():
-            along(tok.at[z], z, step, 0).wait_send()
+            for c in range(parts_n):
+                along(tok.at[z], z, step, 0, c).wait_send()
 
         @pl.when(down_open & (z + step < planes))
         def _():
-            along(tok.at[z], z, step, 1).wait_send()
+            for c in range(parts_n):
+                along(tok.at[z], z, step, 1, c).wait_send()
 
 
 def experts(
@@ -418,8 +437,9 @@
             blocks, blocks,
             pltpu.VMEM((tokens, width), f32),
             pltpu.VMEM((planes // 2, tokens, width), bf16),
-            dma((3,)), dma((2, planes)), dma((2, planes)), dma((2, planes)), dma((2, planes)),
-            dma((planes, near)), dma((planes, near)), dma((planes, near)), dma((planes, near)),
+            dma((3,)), dma((2, planes)), dma((2, planes)),
+            dma((2, planes, 2)), dma((2, planes, 2)), dma((planes, near, 2)),
+            dma((planes, near, 2)), dma((planes, near)), dma((planes, near)),
             dma((planes, width // 512)), dma((planes, width // 512)),
             dma((planes // 2, width // 512)), dma((planes // 2, width // 512)), dma((2, planes)),
         ],
@@ -458,7 +478,7 @@
     taps_n, wide = tx_ref.shape
     half = taps_n // 2
     depth = w_hbm.shape[0]
-    piece = min(depth, 128)
+    piece = min(depth, 64)
     pieces = depth // piece
     bits = [1 << i for i in range(dp_count.bit_length() - 1)]
     flows = (x_hbm, b_hbm, c_hbm)
@@ -513,13 +533,32 @@
             in_s.at[k, q, i], in_r.at[k, q, i], {"sp": z * inner + peer},
         )
 
+    odd_x = lax.rem(x, 2)
+    shared, missing = odd_x * (pieces - 1), (1 - odd_x) * (pieces - 1)
+    across = [o for o in range(2, dp_count, 2)]
+    across = sorted(across, key=lambda o: (-lowest(o), o))
+
     def give_weight(offset, bit, c):
-        rows = slice(c * piece, (c + 1) * piece)
+        rows = spot(c * piece, piece)
         src = w_hbm.at[rows] if offset == 0 else w_all.at[offset, rows]
+        if bit:
+            index, there = bits.index(bit), {"dp": mate(bit)}
+        else:
+            index, there = len(bits), {"sp": sp + 1 - 2 * odd_x}
         return remote(
             src, w_all.at[offset + bit, rows],
-            w_s.at[offset, bits.index(bit), c], w_r.at[offset + bit, c], {"dp": mate(bit)},
-        )
+            w_s.at[offset, index, c], w_r.at[offset + bit, c], there,
+        )
+
+    def weight_in(offset, c):
+        rows = spot(c * piece, piece)
+        remote(
+            w_hbm.at[rows], w_all.at[offset, rows],
+            w_s.at[0, 0, c], w_r.at[offset, c], {"dp": mate(1)},
+        ).wait_recv()
+
+    def between(offset):
+        return [bit for bit in bits if 1 < bit < lowest(offset)]
 
     has_above, has_below = z < planes - 1, z > 0
     sends_up = has_above & (x == inner - 1)
@@ -559,9 +598,11 @@
     ]
     for copy in owned:
         copy.start()
-    for bit in reversed(bits):
-        for c in range(pieces):
+    for c in [shared] + list(range(1, pieces - 1)):
+        for bit in reversed(bits[1:]):
             give_weight(0, bit, c).start()
+    for c in range(pieces):
+        give_weight(0, 1, c).start()
     keeps = [
         pltpu.make_async_copy(tap_refs[k], taps.at[k, 0:taps_n, mine], local.at[k])
         for k in range(3)
@@ -802,6 +843,13 @@
                     give_in(k, t, i).wait_recv()
             local_part(t)
 
+        @pl.when(t == 3 * locals_n // 4)
+        def _():
+            for offset in across:
+                weight_in(offset, shared)
+                for bit in between(offset) + [0, 1]:
+                    give_weight(offset, bit, shared).start()
+
         @pl.when(has_below & (f >= 0) & (f < locals_n))
         def _():
             pass_f(f).wait_recv()
@@ -861,13 +909,11 @@
     lax.fori_loop(0, groups, scale, 0)
 
     stream_ref[...] = res_v[...].astype(f32)
-    order = sorted(range(1, dp_count), key=lambda o: (-lowest(o), o))
-
-    def come(offset, c):
-        give_weight(offset - lowest(offset), lowest(offset), c).wait_recv()
-        for bit in bits:
-            if bit < lowest(offset):
-                give_weight(offset, bit, c).start()
+
+    def come(offset, c, onward):
+        weight_in(offset, c)
+        for bit in onward:
+            give_weight(offset, bit, c).start()
 
     def project(offset, first, last):
         block = dp
@@ -885,16 +931,24 @@
 
         lax.fori_loop(0, width // 512, tile, 0)
 
-    early = depth - piece
-    for offset in order:
-        for c in range(pieces - 1):
-            come(offset, c)
+    early = depth - 2 * piece
+    odd = range(1, dp_count, 2)
+    for offset in across:
+        for c in range(1, pieces - 2):
+            come(offset, c, between(offset) + [1])
+        come(offset, missing, [1])
+    for offset in odd:
+        for c in list(range(pieces - 2)) + [pieces - 1]:
+            come(offset, c, [])
     project(0, 0, depth)
-    for offset in order:
-        if early:
+    if early:
+        for offset in range(1, dp_count):
             project(offset, 0, early)
-    for offset in order:
-        come(offset, pieces - 1)
+    for offset in across:
+        come(offset, pieces - 2, between(offset) + [1])
+        project(offset, early, depth)
+    for offset in odd:
+        come(offset, pieces - 2, [])
         project(offset, early, depth)
     total = jnp.zeros((tokens, 1), f32)
     for at in range(0, width, 512):
@@ -942,11 +996,14 @@
         return unused
 
     lax.fori_loop(0, locals_n, drain, 0)
-    for offset in range(dp_count):
-        for bit in bits:
-            if offset == 0 or bit < lowest(offset):
-                for c in range(pieces):
-                    give_weight(offset, bit, c).wait_send()
+    for offset in [0] + across:
+        for c in [shared] + list(range(1, pieces - 1)):
+            for bit in between(offset) if offset else bits[1:]:
+                give_weight(offset, bit, c).wait_send()
+        for c in range(pieces):
+            give_weight(offset, 1, c).wait_send()
+        if offset:
+            give_weight(offset, 0, shared).wait_send()
 
 
 def mixer(
@@ -960,7 +1017,7 @@
     own = groups // inner
     span = width // inner
     depth = weight.shape[0]
-    pieces = depth // min(depth, 128)
+    pieces = depth // min(depth, 64)
     bits = dp_count.bit_length() - 1
     inside = pl.BlockSpec(memory_space=pltpu.VMEM)
     anywhere = pl.BlockSpec(memory_space=pl.ANY)
@@ -1000,7 +1057,7 @@
             dma((3, n)), dma((3, n)), dma((n,)), dma((n,)), dma((2, 3, inner)), dma((2, 3)),
             dma((own,)), dma((own,)), dma((own,)), dma((own,)),
             dma((inner, own)), dma((inner, own)),
-            dma((dp_count, bits, pieces)), dma((dp_count, pieces)), dma((3,)), dma((8,)),
+            dma((dp_count, bits + 1, pieces)), dma((dp_count, pieces)), dma((3,)), dma((8,)),
         ],
         compiler_params=pltpu.CompilerParams(
             collective_id=1, has_side_effects=True, vmem_limit_bytes=56 * 1024 * 1024

time: 171 us -> 167 us (0.977)
  Pallas kernels: 167 us -> 162 us
    pallas_call x1, Pallas kernels: 111 us -> 107 us  [experts(): pl.pallas_call(functools.partial(experts_kernel, planes, inner, dp_count,...]
where the time goes in v5:
time: 167 us; the launch traced here: 164 us
  Pallas kernels  162 us (97%)
  local copies, waits for them, and re-layouts  1.88 us (1%)
    pallas_call x1, Pallas kernels, experts(): pl.pallas_call(functools.partial(experts_kernel, planes, inner, dp_count,...  107 us
    pallas_call x1, Pallas kernels, mixer(): pl.pallas_call(functools.partial(mixer_kernel, n, inner, dp_count), out_s...  54.9 us

profile of v5, /device:TPU:29, one launch (start us, length us, event | category | flops | bytes accessed | tf_op | source)
XLA Modules:
  0.0 163.6 jit_solution(16830262259608625179)
XLA Ops:
  0.0 54.9 %mixer.1 = (f32[128,2048]{1,0:T(8,128)}, bf16[128,2048]{1,0:T(8,128)(2,1)}) custom-call(bf16[128,2048]{1,0:T(8,128)(2,1)} %bitcast.18, bf16[128,2048]{1,0:T(8,128)(2,1)} %bitcast.19, bf16[128,2048]{1,0:T(8,128)(2,1)} %bitcast.20, bf16[128,2048]{1,0:T(8,128)(2,1)} %bitcast.21, bf16[128,2048]{1,0:T(8,128)(2,1)} %bitcast.22, bf16[512,2048]{1,0:T(8,128)(2,1)} %w_hbm.1, ...), custom_call_target="tpu_custom_call" | custom-call | flops 40000000000 | bytes 2097152 | tf_op jit(solution)/shard_map/mixer/pallas_call | solution.py:1030
  54.9 106.8 %experts.1 = bf16[128,2048]{1,0:T(8,128)(2,1)} custom-call(bf16[128,2048]{1,0:T(8,128)(2,1)} %get-tuple-element.7.x_ref, f32[128,2048]{1,0:T(8,128)} %get-tuple-element.8.stream_ref, s32[4,128]{1,0:T(4,128)} %bitcast.26, f32[4,128]{1,0:T(4,128)} %bitcast.27, bf16[1,2048,1024]{2,1,0:T(8,128)(2,1)} %gate_hbm.1, bf16[1,2048,1024]{2,1,0:T(8,128)(2,1)} %up_hbm.1, ...), custom_call_target="tpu_custom_call" | custom-call | flops 99999997952 | bytes 100000000 | tf_op jit(solution)/shard_map/experts/pallas_call | solution.py:423
  161.7 1.9 %copy.20 = bf16[1,128,2048]{2,1,0:T(8,128)(2,1)} copy(bf16[1,128,2048]{2,1,0:T(8,128)(2,1)} %bitcast.17) | data formatting | bytes 1048576

commit v6 on v5

--- a/solution.py
+++ b/solution.py
@@ -836,35 +836,35 @@
     def turn(t, unused):
         f, b, g = t - late_f, t - late_b, t - late
 
+        @pl.when(t == 3 * locals_n // 4)
+        def _():
+            for offset in across:
+                weight_in(offset, shared)
+                for bit in between(offset) + [0, 1]:
+                    give_weight(offset, bit, shared).start()
+
+        @pl.when(has_below & (f >= 0) & (f < locals_n))
+        def _():
+            pass_f(f).wait_recv()
+
+            @pl.when(has_above)
+            def _():
+                onward_f(f, got_f[f].astype(f32))
+
+        @pl.when(has_above & (b >= 0) & (b < locals_n))
+        def _():
+            pass_b(b).wait_recv()
+
+            @pl.when(has_below)
+            def _():
+                onward_b(b, got_b[b].astype(f32))
+
         @pl.when(t < locals_n)
         def _():
             for k in range(3):
                 for i in range(1, inner):
                     give_in(k, t, i).wait_recv()
             local_part(t)
-
-        @pl.when(t == 3 * locals_n // 4)
-        def _():
-            for offset in across:
-                weight_in(offset, shared)
-                for bit in between(offset) + [0, 1]:
-                    give_weight(offset, bit, shared).start()
-
-        @pl.when(has_below & (f >= 0) & (f < locals_n))
-        def _():
-            pass_f(f).wait_recv()
-
-            @pl.when(has_above)
-            def _():
-                onward_f(f, got_f[f].astype(f32))
-
-        @pl.when(has_above & (b >= 0) & (b < locals_n))
-        def _():
-            pass_b(b).wait_recv()
-
-            @pl.when(has_below)
-            def _():
-                onward_b(b, got_b[b].astype(f32))
 
         @pl.when((g >= 0) & (g < locals_n))
         def _():

time: 167 us -> 166 us (level)
  no operation moved by 1% of the time
where the time goes in v6:
time: 166 us; the launch traced here: 164 us
  Pallas kernels  162 us (98%)
  local copies, waits for them, and re-layouts  1.88 us (1%)
    pallas_call x1, Pallas kernels, experts(): pl.pallas_call(functools.partial(experts_kernel, planes, inner, dp_count,...  107 us
    pallas_call x1, Pallas kernels, mixer(): pl.pallas_call(functools.partial(mixer_kernel, n, inner, dp_count), out_s...  54.9 us

profile of v6, /device:TPU:29, one launch (start us, length us, event | category | flops | bytes accessed | tf_op | source)
XLA Modules:
  0.0 163.6 jit_solution(921560592190539526)
XLA Ops:
  0.0 54.9 %mixer.1 = (f32[128,2048]{1,0:T(8,128)}, bf16[128,2048]{1,0:T(8,128)(2,1)}) custom-call(bf16[128,2048]{1,0:T(8,128)(2,1)} %bitcast.18, bf16[128,2048]{1,0:T(8,128)(2,1)} %bitcast.19, bf16[128,2048]{1,0:T(8,128)(2,1)} %bitcast.20, bf16[128,2048]{1,0:T(8,128)(2,1)} %bitcast.21, bf16[128,2048]{1,0:T(8,128)(2,1)} %bitcast.22, bf16[512,2048]{1,0:T(8,128)(2,1)} %w_hbm.1, ...), custom_call_target="tpu_custom_call" | custom-call | flops 40000000000 | bytes 2097152 | tf_op jit(solution)/shard_map/mixer/pallas_call | solution.py:1030
  54.9 106.8 %experts.1 = bf16[128,2048]{1,0:T(8,128)(2,1)} custom-call(bf16[128,2048]{1,0:T(8,128)(2,1)} %get-tuple-element.7.x_ref, f32[128,2048]{1,0:T(8,128)} %get-tuple-element.8.stream_ref, s32[4,128]{1,0:T(4,128)} %bitcast.26, f32[4,128]{1,0:T(4,128)} %bitcast.27, bf16[1,2048,1024]{2,1,0:T(8,128)(2,1)} %gate_hbm.1, bf16[1,2048,1024]{2,1,0:T(8,128)(2,1)} %up_hbm.1, ...), custom_call_target="tpu_custom_call" | custom-call | flops 99999997952 | bytes 100000000 | tf_op jit(solution)/shard_map/experts/pallas_call | solution.py:423
  161.7 1.9 %copy.20 = bf16[1,128,2048]{2,1,0:T(8,128)(2,1)} copy(bf16[1,128,2048]{2,1,0:T(8,128)(2,1)} %bitcast.17) | data formatting | bytes 1048576
